TPU v7x, 32 devices: a whole 2x2x4 slice. The times are simulated.
32 devices in a mesh: sp: 8 (over z, y), dp: 4 (over x, core).
Axes of the slice: x: 2, y: 2, z: 4, core: 2. Of those that a mesh axis runs over, the one named last changes fastest.
Arguments:
- query: bfloat16 [4, 1536, 3072], P('dp', 'sp'), may hold values from -18 to 18
- latent: bfloat16 [4, 1536, 1024], P('dp', 'sp'), may hold values from -6 to 6
- rope_key: bfloat16 [4, 1536, 32], P('dp', 'sp'), may hold values from -5 to 5
- latent_norm_gain: float32 [1024], replicated, may hold values from 0.1 to 1.9
- key_up_matrix: bfloat16 [2048, 1024], P('dp'), may hold values from -0.1875 to 0.1875
- value_up_matrix: bfloat16 [2048, 1024], P('dp'), may hold values from -0.1875 to 0.1875
- out_grad: bfloat16 [4, 1536, 2048], P('dp', 'sp'), may hold values from -6 to 6
Outputs:
- query_grad: bfloat16 [4, 1536, 3072], P('dp', 'sp')
- latent_grad: float32 [4, 1536, 1024], P('dp', 'sp')
- rope_key_grad: float32 [4, 1536, 32], P('dp', 'sp')
- key_weight_grad: float32 [2048, 1024], P('dp')
- value_weight_grad: float32 [2048, 1024], P('dp')
- gain_grad: float32 [1024], replicated
All inputs are finite; a program needn't handle non-finite values.
Results may differ from a plain program's by a relative error of at most 0.011.
Values may be sent and summed in bfloat16 or wider, within the bound.
A program may use at most 256 MiB of HBM per device.

v0:
```python
import jax
import jax.numpy as jnp
from jax import lax
from jax.sharding import PartitionSpec as P

ATTENTION_HEADS = 32
PLAIN_HEAD_WIDTH = 64
ROPE = 32
VALUE_HEAD_WIDTH = 64
SPAN = 64


eps = 1e-06
rope_base = 10000.0


def rotate(values, cosine, sine):
    half = values.shape[-1] // 2
    first = values[..., :half]
    second = values[..., half:]
    return jnp.concatenate(
        [first * cosine - second * sine, second * cosine + first * sine], axis=-1
    )


def angles(length, width):
    inverse = 1.0 / rope_base ** (jnp.arange(0, width, 2, dtype=jnp.float32) / width)
    turned = jnp.arange(length, dtype=jnp.float32)[:, None] * inverse[None, :]
    return (jnp.cos(turned), jnp.sin(turned))


def attend_backward(arrived, rope_full):
    f32 = jnp.float32
    bf16 = jnp.bfloat16
    length = arrived.shape[0]
    local_heads = arrived.shape[1]
    width = PLAIN_HEAD_WIDTH + ROPE
    scale = width ** (-0.5)
    block = 512
    cosine, sine = angles(length, ROPE)
    neg = jnp.finfo(f32).min
    q_nope = arrived[:, :, :PLAIN_HEAD_WIDTH]
    q_rope = rotate(
        arrived[:, :, PLAIN_HEAD_WIDTH:width].astype(f32), cosine[:, None, :], sine[:, None, :]
    ).astype(bf16)
    key_nope = arrived[:, :, width : width + PLAIN_HEAD_WIDTH]
    values = arrived[:, :, width + PLAIN_HEAD_WIDTH : width + PLAIN_HEAD_WIDTH + VALUE_HEAD_WIDTH]
    d_out = arrived[:, :, width + PLAIN_HEAD_WIDTH + VALUE_HEAD_WIDTH :]
    k_rope = rotate(rope_full.astype(f32), cosine, sine).astype(bf16)
    dk_nope = jnp.zeros((length, local_heads, PLAIN_HEAD_WIDTH), f32)
    dk_rope = jnp.zeros((length, ROPE), f32)
    d_vals = jnp.zeros((length, local_heads, VALUE_HEAD_WIDTH), f32)
    dq_parts = []
    for begin in range(0, length, block):
        end = begin + block
        qn = q_nope[begin:end]
        qr = q_rope[begin:end]
        go = d_out[begin:end]
        scores = jnp.einsum("qhd,khd->hqk", qn, key_nope[:end], preferred_element_type=f32)
        scores = (
            scores + jnp.einsum("qhd,kd->hqk", qr, k_rope[:end], preferred_element_type=f32)
        ) * scale
        q_seg = jnp.arange(begin, end) // SPAN
        k_seg = jnp.arange(end) // SPAN
        allowed = k_seg[None, :] <= q_seg[:, None]
        scores = jnp.where(allowed[None], scores, neg)
        probs = jax.nn.softmax(scores, axis=-1)
        d_probs = jnp.einsum("qhd,khd->hqk", go, values[:end], preferred_element_type=f32)
        d_scores = probs * (d_probs - jnp.sum(probs * d_probs, axis=-1, keepdims=True))
        ds_b = d_scores.astype(bf16)
        p_b = probs.astype(bf16)
        dq_n = jnp.einsum("hqk,khd->qhd", ds_b, key_nope[:end], preferred_element_type=f32) * scale
        dq_r = jnp.einsum("hqk,kd->qhd", ds_b, k_rope[:end], preferred_element_type=f32) * scale
        dq_r = rotate(dq_r, cosine[begin:end, None, :], -sine[begin:end, None, :])
        dq_parts.append(jnp.concatenate([dq_n, dq_r], axis=-1).astype(bf16))
        dk_nope = dk_nope.at[:end].add(
            jnp.einsum("hqk,qhd->khd", ds_b, qn, preferred_element_type=f32) * scale
        )
        dk_rope = dk_rope.at[:end].add(
            jnp.einsum("hqk,qhd->kd", ds_b, qr, preferred_element_type=f32) * scale
        )
        d_vals = d_vals.at[:end].add(
            jnp.einsum("hqk,qhd->khd", p_b, go, preferred_element_type=f32)
        )
    query_part = jnp.concatenate(dq_parts, axis=0)
    grads = jnp.concatenate([query_part, dk_nope.astype(bf16), d_vals.astype(bf16)], axis=-1)
    return (grads, rotate(dk_rope, cosine, -sine))


def local(query, latent, rope_key, latent_norm_gain, key_up_matrix, value_up_matrix, out_grad):
    f32 = jnp.float32
    bf16 = jnp.bfloat16
    tokens = latent.shape[1]
    width = PLAIN_HEAD_WIDTH + ROPE
    head_cols = ATTENTION_HEADS * PLAIN_HEAD_WIDTH
    lat = latent[0].astype(f32)
    inv_rms = lax.rsqrt(jnp.mean(lat * lat, axis=-1, keepdims=True) + eps)
    normed = lat * inv_rms
    nlat = (normed * latent_norm_gain).astype(bf16)
    stacked = jnp.stack([key_up_matrix, value_up_matrix])
    whole = lax.all_gather(stacked, "dp", axis=1, tiled=True)
    kv_tok = jnp.einsum("tc,gnc->tgn", nlat, whole, preferred_element_type=f32).astype(bf16)
    heads_query = query[0].reshape(tokens, ATTENTION_HEADS, width)
    key_nope = kv_tok[:, 0].reshape(tokens, ATTENTION_HEADS, PLAIN_HEAD_WIDTH)
    values = kv_tok[:, 1].reshape(tokens, ATTENTION_HEADS, VALUE_HEAD_WIDTH)
    d_out = out_grad[0].reshape(tokens, ATTENTION_HEADS, VALUE_HEAD_WIDTH)
    packed = jnp.concatenate([heads_query, key_nope, values, d_out], axis=2)
    arrived = lax.all_to_all(packed, "sp", split_axis=1, concat_axis=0, tiled=True)
    rope_full = lax.all_gather(rope_key[0], "sp", axis=0, tiled=True)
    grads_heads, rope_full_grad = attend_backward(arrived, rope_full)
    returned = lax.all_to_all(grads_heads, "sp", split_axis=0, concat_axis=1, tiled=True)
    rope_grad = lax.psum_scatter(rope_full_grad, "sp", scatter_dimension=0, tiled=True)
    query_grad = returned[:, :, :width].reshape(tokens, ATTENTION_HEADS * width)
    key_cols = returned[:, :, width : width + PLAIN_HEAD_WIDTH].reshape(tokens, head_cols)
    value_cols = returned[:, :, width + PLAIN_HEAD_WIDTH :].reshape(tokens, head_cols)
    dkv = jnp.stack([key_cols, value_cols], axis=1)
    d_nlat = jnp.einsum("tgn,gnc->tc", dkv, whole, preferred_element_type=f32)
    latents_all = lax.all_gather(nlat[None], "dp", axis=0, tiled=True)
    columns = lax.all_to_all(dkv[None], "dp", split_axis=3, concat_axis=0, tiled=True)
    partial_value = jnp.einsum("stgr,stc->grc", columns, latents_all, preferred_element_type=f32)
    weight_grads = lax.psum(partial_value, "sp")
    gain_grad = lax.psum(jnp.sum(d_nlat * normed, axis=0), ("sp", "dp"))
    scaled = d_nlat * latent_norm_gain
    latent_grad = inv_rms * (scaled - normed * jnp.mean(scaled * normed, axis=-1, keepdims=True))
    return (
        query_grad[None],
        latent_grad[None],
        rope_grad[None],
        weight_grads[0],
        weight_grads[1],
        gain_grad,
    )


def solution(mesh):
    in_specs = (
        P("dp", "sp", None),
        P("dp", "sp", None),
        P("dp", "sp", None),
        P(),
        P("dp", None),
        P("dp", None),
        P("dp", "sp", None),
    )
    out_specs = (
        P("dp", "sp", None),
        P("dp", "sp", None),
        P("dp", "sp", None),
        P("dp", None),
        P("dp", None),
        P(),
    )
    return jax.shard_map(local, mesh=mesh, in_specs=in_specs, out_specs=out_specs, check_vma=False)
```

profile of v0, /device:TPU:0, one launch (start us, length us, event | category | flops | bytes accessed | tf_op | source)
XLA Modules:
  0.0 738.0 jit_solution(6265751976223707838)
XLA Ops:
  7.2 3.1 pad_maximum_fusion.2
  10.9 1.4 copy.96
  12.3 3.9 reshape_squeeze.12
  16.4 55.1 %all-gather.4.cloned.1.call-done = bf16[2,2048,1024]{2,1,0:T(8,128)(2,1)} async-done(((bf16[2,512,1024]{2,1,0:T(8,128)(2,1)}), bf16[2,2048,1024]{2,1,0:T(8,128)(2,1)}) %all-gather.4.cloned.1.call-update) | async-done | bytes 8388624 | tf_op jit(solution)/shard_map/all_gather | solution.py:101
  71.5 6.2 convolution_convert_fusion
  80.0 2.4 copy.94
  82.4 2.2 copy.92
  84.6 3.1 copy.95
  87.8 5.6 pad_maximum_fusion
  93.4 4.0 copy.97
  97.4 5.6 all-to-all-start
  103.2 126.8 %all-gather = bf16[1,1536,32]{2,0,1:T(2,128)(2,1)S(1)} all-gather(bf16[1,192,32]{2,0,1:T(2,128)(2,1)S(1)} %copy.99), channel_id=2, replica_groups=mesh['sp'=8,'dp'=4] {'sp'}, dimensions={1}, use_global_device_ids=true | all-gather | bytes 110592 | tf_op jit(solution)/shard_map/all_gather | solution.py:109
  235.0 1.4 broadcast_compare_fusion
  236.4 8.3 %copy.98 = bf16[8,192,4,288]{1,0,3,2:T(8,128)(2,1)} copy(bf16[8,192,4,288]{3,1,2,0:T(8,128)(2,1)} %bitcast.8) | data formatting | bytes 7077888 | tf_op jit(solution)/shard_map/all_to_all | solution.py:108
  244.7 6.9 all_to_all.42
  254.7 3.3 fusion.152
  258.0 5.4 fusion.43
  263.4 3.1 multiply_reduce_fusion.2
  269.2 2.1 fusion.51
  271.3 1.7 fusion.46
  274.4 3.2 fusion.6
  277.6 2.0 fusion.153
  280.8 2.8 multiply_reduce_fusion.1
  283.7 9.7 %multiply_convert_fusion.1 = bf16[4,512,1024]{2,1,0:T(8,128)(2,1)S(1)} fusion(f32[4,512,1024]{2,1,0:T(8,128)S(1)} %get-tuple-element.177, f32[4,512]{1,0:T(4,128)S(1)} %get-tuple-element.176, f32[4,512,1024]{2,1,0:T(8,128)S(1)} %get-tuple-element.171, f32[4,512]{1,0:T(4,128)S(1)} %get-tuple-element.170), kind=kLoop, calls=%fused_computation.12 | loop fusion | flops 8388608 | bytes 20987904 | tf_op jit(solution)/shard_map/convert_element_type | solution.py:70
  293.4 2.1 fusion.54
  295.5 3.1 fusion.50
  298.7 1.8 fusion.114
  300.5 8.5 %fusion.4 = f32[4,512,1536]{2,1,0:T(8,128)} fusion(f32[1536,512,4]{0,1,2:T(8,128)S(1)} %fusion.114, pred[512,1536]{1,0:T(8,128)(4,1)S(1)} %copy-done.13, bf16[1536,4,288]{0,2,1:T(8,128)(2,1)} %copy-done.3), kind=kOutput, calls=%fused_computation.5 | convolution fusion | flops 412090368 | bytes 27000832 | tf_op jit(solution)/shard_map/qhd,khd->hqk/dot_general | solution.py:59
  309.1 14.9 %fusion.154 = (f32[4,512]{1,0:T(4,128)S(1)}, f32[4,512,1536]{2,1,0:T(8,128)}) fusion(f32[4,512,1536]{2,1,0:T(8,128)} %fusion.4), kind=kOutput, calls=%fused_computation.226 | output fusion | flops 6292991 | bytes 25174016 | tf_op jit(solution)/shard_map/sub | solution.py:67
  323.9 11.8 %multiply_reduce_fusion = (f32[4,512]{1,0:T(4,128)S(1)}, f32[4,512,1536]{2,1,0:T(8,128)}) fusion(f32[4,512,1536]{2,1,0:T(8,128)} %get-tuple-element.173, f32[4,512]{1,0:T(4,128)S(1)} %get-tuple-element.172, bf16[1536,4,288]{0,2,1:T(8,128)(2,1)} %copy-done.3), kind=kOutput, calls=%fused_computation.7 | convolution fusion | flops 412088320 | bytes 26230784 | tf_op jit(solution)/shard_map/qhd,khd->hqk/dot_general | solution.py:68
  335.7 6.0 multiply_convert_fusion
  341.8 4.5 fusion.52
  346.3 2.7 fusion.53
  348.9 1.3 scatter-add.24
  350.3 1.3 scatter-add.20
  351.6 11.2 %fusion.37 = f32[1536,4,64]{0,2,1:T(8,128)} fusion(f32[1536,4,64]{0,2,1:T(8,128)} %scatter-add.24, bf16[1536,4,288]{0,2,1:T(8,128)(2,1)} %copy-done.3, f32[4,512]{1,0:T(4,128)S(1)} %get-tuple-element.170, f32[4,512,1024]{2,1,0:T(8,128)} %copy-done.2), kind=kOutput, calls=%fused_computation.53 | convolution fusion | flops 274992128 | bytes 19144704 | tf_op jit(solution)/shard_map/hqk,qhd->khd/dot_general | solution.py:83
  362.8 4.4 fusion.42
  367.2 13.7 %fusion.22 = bf16[1536,4,64]{0,2,1:T(8,128)(2,1)} fusion(f32[1536,4,64]{0,2,1:T(8,128)} %fusion.37, bf16[1536,4,288]{0,2,1:T(8,128)(2,1)} %copy-done.3, f32[4,512]{1,0:T(4,128)S(1)} %get-tuple-element.172, f32[4,512,1536]{2,1,0:T(8,128)} %fusion.4), kind=kOutput, calls=%fused_computation.36 | convolution fusion | flops 412880384 | bytes 27795456 | tf_op jit(solution)/shard_map/hqk,qhd->khd/dot_general | solution.py:83
  381.0 4.6 fusion.21
  385.9 3.0 pad_maximum_fusion.1
  388.8 5.8 copy.107
  394.6 4.6 all-to-all-start.1
  401.9 64.4 %all-to-all-done.1 = bf16[1536,4,224]{2,1,0:T(4,128)(2,1)} async-done(((bf16[1536,4,224]{2,1,0:T(4,128)(2,1)}), bf16[1536,4,224]{2,1,0:T(4,128)(2,1)}, u32[]{:S(2)}, u32[]{:S(2)}) %all-to-all-start.1) | async-done | bytes 2752544 | tf_op jit(solution)/shard_map/all_to_all | solution.py:111
  466.3 2.3 copy.108
  468.8 2.8 fusion.149
  471.5 2.6 copy.111
  474.1 2.2 copy.113
  476.3 2.6 copy.112
  478.9 2.2 copy.114
  481.1 2.7 fusion.60
  483.8 6.1 copy.116
  489.8 4.4 all-to-all-start.2
  494.3 3.7 fusion.58
  498.0 4.0 fusion.26
  503.7 16.3 %all-to-all-done.2 = bf16[1,192,2,2048]{1,2,0,3:T(2,128)(2,1)} async-done(((bf16[1,192,2,2048]{1,2,0,3:T(2,128)(2,1)}), bf16[1,192,2,2048]{1,2,0,3:T(2,128)(2,1)}, u32[]{:S(2)}, u32[]{:S(2)}) %all-to-all-start.2) | async-done | bytes 1572896 | tf_op jit(solution)/shard_map/all_to_all | solution.py:119
  520.0 6.0 copy.118
  526.0 5.7 convolution_bitcast_fusion.1
  531.7 34.6 %reduce-scatter.4.cloned.1.call-done = f32[192,32]{1,0:T(8,128)} async-done(((f32[1536,32]{1,0:T(8,128)}), f32[192,32]{1,0:T(8,128)}) %reduce-scatter.4.cloned.1.call-update) | async-done | bytes 24592
  566.3 1.6 copy.130
  569.2 3.0 broadcast_in_dim_reshape.3
  572.2 6.3 fusion.72
  578.5 44.0 %psum.15 = f32[1024]{0:T(1024)} all-reduce(f32[1024]{0:T(1024)S(1)} %get-tuple-element.138), channel_id=1, replica_groups=mesh['sp'=8,'dp'=4] {'sp','dp'}, use_global_device_ids=true, to_apply=%region_14.15 | all-reduce | flops 1024 | bytes 8192 | tf_op jit(solution)/shard_map/psum | solution.py:122
  623.6 102.6 %all-reduce.5.cloned.1.call-done = f32[2,512,1024]{2,1,0:T(8,128)} async-done(((f32[2,512,1024]{2,1,0:T(8,128)}), f32[2,512,1024]{2,1,0:T(8,128)}) %all-reduce.5.cloned.1.call-update) | async-done | bytes 4194320 | tf_op jit(solution)/shard_map/psum | solution.py:121
  726.2 4.8 slice_bitcast_fusion
  (152 shorter events, 23.7 us)
Async XLA Ops:
  7.2 3.2 copy-start.32
  7.2 64.3 %all-gather.4.cloned.1.call-start = ((), (), s32[]{:S(2)}) async-start(), calls=%async_computation.4 | async-start | bytes 10485760 | tf_op jit(solution)/shard_map/all_gather | solution.py:101
  10.3 5.9 copy-start.10
  10.4 61.1 %copy-start.41 = (f32[1024]{0:T(1024)S(1)}, f32[1024]{0:T(1024)}, u32[]{:S(2)}) copy-start(f32[1024]{0:T(1024)} %param.34) | copy-start | bytes 12292
  16.4 55.1 %copy-start.44 = (f32[192]{0:T(256)}, f32[192]{0:T(256)S(1)}, u32[]{:S(2)}) copy-start(f32[192]{0:T(256)S(1)} %add_rsqrt_fusion) | copy-start | bytes 2308
  97.4 5.7 copy-start.43
  97.4 139.0 %all-to-all-start = ((bf16[192,32,288]{2,0,1:T(8,128)(2,1)}), bf16[192,32,288]{2,0,1:T(8,128)(2,1)}, u32[]{:S(2)}, u32[]{:S(2)}) async-start(bf16[192,32,288]{2,0,1:T(8,128)(2,1)} %copy.97), calls=%async_computation | async-start | bytes 9437184 | tf_op jit(solution)/shard_map/all_to_all | solution.py:108
  230.4 1.2 copy-start.46
  231.6 0.6 copy-start.28
  231.6 0.7 copy-start.30
  251.6 11.8 %copy-start.3 = (bf16[1536,4,288]{0,2,1:T(8,128)(2,1)}, bf16[1536,4,288]{0,2,1:T(8,128)(2,1)S(1)}, u32[]{:S(2)}) copy-start(bf16[1536,4,288]{0,2,1:T(8,128)(2,1)S(1)} %all_to_all.42) | copy-start | bytes 10616836
  251.6 1.0 copy-start.29
  251.6 1.1 copy-start.31
  251.6 2.0 copy-start.16
  251.6 2.0 copy-start.18
  251.6 2.0 copy-start.24
  252.8 0.7 copy-start.6
  252.8 0.8 copy-start.8
  254.7 3.3 copy-start.5
  263.4 3.4 copy-start.4
  266.8 1.2 copy-start.17
  266.8 1.2 copy-start.19
  268.0 5.0 copy-start.7
  268.0 5.0 copy-start.9
  273.0 1.3 copy-start.20
  277.6 3.3 copy-start.2
  293.4 5.2 copy-start.1
  298.7 1.8 copy-start.13
  323.9 11.8 %slice-start = ((s8[12582912]{0:T(1024)(128)(4,1)}), s8[4194304]{0:T(1024)(128)(4,1)S(1)}, s32[]{:S(2)}) async-start(s8[12582912]{0:T(1024)(128)(4,1)} %bitcast.187), calls=%async_computation.8 | async-start | bytes 8388608
  323.9 11.8 %slice-start.1 = ((s8[12582912]{0:T(1024)(128)(4,1)}), s8[4194304]{0:T(1024)(128)(4,1)S(1)}, s32[]{:S(2)}) async-start(s8[12582912]{0:T(1024)(128)(4,1)} %bitcast.187), calls=%async_computation.9 | async-start | bytes 8388608
  323.9 11.8 %slice-start.2 = ((s8[12582912]{0:T(1024)(128)(4,1)}), s8[4194304]{0:T(1024)(128)(4,1)S(1)}, s32[]{:S(2)}) async-start(s8[12582912]{0:T(1024)(128)(4,1)} %bitcast.187), calls=%async_computation.10 | async-start | bytes 8388608
  341.8 7.1 copy-start
  346.3 2.7 copy-start.34
  380.9 4.7 copy-start.21
  380.9 4.8 copy-start.39
  380.9 4.8 copy-start.40
  380.9 4.8 copy-start.22
  380.9 4.8 copy-start.37
  380.9 4.8 copy-start.38
  380.9 4.9 copy-start.23
  380.9 4.9 copy-start.35
  380.9 4.9 copy-start.36
  380.9 4.9 copy-start.25
  381.0 4.9 copy-start.26
  381.0 4.9 copy-start.27
  381.0 4.9 copy-start.33
  394.6 4.9 copy-start.11
  394.6 4.9 copy-start.42
  394.6 4.9 copy-start.45
  394.6 71.6 %all-to-all-start.1 = ((bf16[1536,4,224]{2,1,0:T(4,128)(2,1)}), bf16[1536,4,224]{2,1,0:T(4,128)(2,1)}, u32[]{:S(2)}, u32[]{:S(2)}) async-start(bf16[1536,4,224]{2,1,0:T(4,128)(2,1)} %copy.107), calls=%async_computation.1 | async-start | bytes 6291456 | tf_op jit(solution)/shard_map/all_to_all | solution.py:111
  399.2 126.8 %all-gather.6.cloned.1.call-start = ((), (), s32[]{:S(2)}) async-start(), calls=%async_computation.5 | async-start | bytes 1966080 | tf_op jit(solution)/shard_map/all_gather | solution.py:118
  489.8 30.2 %all-to-all-start.2 = ((bf16[1,192,2,2048]{1,2,0,3:T(2,128)(2,1)}), bf16[1,192,2,2048]{1,2,0,3:T(2,128)(2,1)}, u32[]{:S(2)}, u32[]{:S(2)}) async-start(bf16[1,192,2,2048]{1,2,0,3:T(2,128)(2,1)} %copy.116), calls=%async_computation.2 | async-start | bytes 4194304 | tf_op jit(solution)/shard_map/all_to_all | solution.py:119
  494.3 72.0 %reduce-scatter.4.cloned.1.call-start = ((), (), s32[]{:S(2)}) async-start(), calls=%async_computation.7 | async-start | bytes 884736
  498.0 4.0 copy-start.47
  503.6 222.6 %all-reduce.5.cloned.1.call-start = ((), (), s32[]{:S(2)}) async-start(), calls=%async_computation.6 | async-start | bytes 8388608 | tf_op jit(solution)/shard_map/psum | solution.py:121
  567.9 4.3 copy-start.12
  568.2 4.0 copy-start.14
  568.2 4.0 copy-start.15
Sparse Core Ops, SparseCore 0:
  10.5 60.9 all-gather.3
  401.6 19.9 all-gather.5
  503.8 62.4 reduce-scatter.3
  569.8 156.3 all-reduce.4
where the time goes:
time: 747 us; the launch traced here: 738 us
  waiting for transfers between devices  273 us (37%)
  blocking collectives  171 us (23%)
  matrix products  118 us (16%)
  local copies, waits for them, and re-layouts  87 us (12%)
  other arithmetic  59.6 us (8%)
  starting transfers between devices  15.1 us (2%)
  between operations  15 us (2%)
    all_gather x1, blocking collectives, local(): rope_full = lax.all_gather(rope_key[0], 'sp', axis=0, tiled=True)  127 us
    psum x1, waiting for transfers between devices, local(): weight_grads = lax.psum(partial_value, 'sp')  103 us
    all_to_all x1, waiting for transfers between devices, local(): lax.all_to_all(grads_heads, 'sp', split_axis=0, concat_axis=1, tiled=True)  64.4 us
    all_gather x1, waiting for transfers between devices, local(): whole = lax.all_gather(stacked, 'dp', axis=1, tiled=True)  55.1 us
    psum x1, blocking collectives, local(): gain_grad = lax.psum(jnp.sum(d_nlat * normed, axis=0), ('sp', 'dp'))  44 us
    unnamed x5, waiting for transfers between devices  34.6 us
    dot_general x3, matrix products, attend_backward(): jnp.einsum('hqk,qhd->khd', p_b, go, preferred_element_type=f32)  30.3 us
    sub x3, other arithmetic, attend_backward(): probs = jax.nn.softmax(scores, axis=-1)  20.1 us
  transfers between devices with their start and end apart: 7, of which 5 were waited for; matrix products, arithmetic and copies ran while one was open for 10% of the time, Pallas kernels for 0%

commit v1 on v0

v1 whole, which is shorter than its diff:
```python
import functools
import math

import jax
import jax.numpy as jnp
from jax import lax
from jax.experimental import pallas as pl
from jax.experimental.pallas import tpu as pltpu
from jax.sharding import PartitionSpec as P

ATTENTION_HEADS = 32
PLAIN_HEAD_WIDTH = 64
ROPE = 32
VALUE_HEAD_WIDTH = 64
SPAN = 64
WIDTH = PLAIN_HEAD_WIDTH + ROPE
LANES = 128

eps = 1e-06
rope_base = 10000.0


def rotate(values, cosine, sine):
    half = values.shape[-1] // 2
    first = values[..., :half]
    second = values[..., half:]
    return jnp.concatenate(
        [first * cosine - second * sine, second * cosine + first * sine], axis=-1
    )


def angles(length, width):
    inverse = 1.0 / rope_base ** (jnp.arange(0, width, 2, dtype=jnp.float32) / width)
    turned = jnp.arange(length, dtype=jnp.float32)[:, None] * inverse[None, :]
    return (jnp.cos(turned), jnp.sin(turned))


NT = (((1,), (1,)), ((), ()))
NN = (((1,), (0,)), ((), ()))


def mm(a, b, dims=NN):
    return lax.dot_general(a, b, dims, preferred_element_type=jnp.float32)


def attention_kernel(
    heads, tile,
    arrived, keys, values, k_rope, cosine, sine,
    dq_out, dkv_out, dr_out,
    q_s, go_s, k_s, kt_s, v_s, s_s, dp_s, dk_s, dv_s, dq_s,
):
    f32 = jnp.float32
    bf16 = jnp.bfloat16
    length = k_rope.shape[0]
    blocks = length // tile
    scale = WIDTH ** (-0.5)
    steep = scale * math.log2(math.e)
    half = ROPE // 2
    pid = pl.program_id(0)

    for h in range(heads):
        @pl.when(pid == h)
        def _():
            raw = arrived[:, h * WIDTH : (h + 1) * WIDTH]
            turned = rotate(
                raw[:, PLAIN_HEAD_WIDTH:].astype(f32), cosine[:, :half], sine[:, :half]
            ).astype(bf16)
            q_s[...] = jnp.concatenate([raw[:, :PLAIN_HEAD_WIDTH], turned], axis=1)
            base = heads * WIDTH + h * VALUE_HEAD_WIDTH
            go_s[...] = arrived[:, base : base + VALUE_HEAD_WIDTH]
            both = jnp.concatenate(
                [keys[:, h * PLAIN_HEAD_WIDTH : (h + 1) * PLAIN_HEAD_WIDTH], k_rope[...]], axis=1
            )
            k_s[...] = both
            v_s[...] = values[:, h * VALUE_HEAD_WIDTH : (h + 1) * VALUE_HEAD_WIDTH]

    for b in range(blocks):
        kt_s[b] = k_s[b * tile : (b + 1) * tile, :].astype(f32).T.astype(bf16)
    dk_s[...] = jnp.zeros_like(dk_s)
    dv_s[...] = jnp.zeros_like(dv_s)

    key_seg = lax.broadcasted_iota(jnp.int32, (tile, tile), 0) // SPAN
    query_seg = lax.broadcasted_iota(jnp.int32, (tile, tile), 1) // SPAN

    def fold(x, op):
        return op(x.reshape(tile // 8, 8, tile), axis=0)

    def query_block(qi, _):
        rows = pl.ds(pl.multiple_of(qi * tile, tile), tile)
        q = q_s[rows, :]
        go = go_s[rows, :]

        def score(kb, peak, diagonal=False):
            at = pl.ds(pl.multiple_of(kb * tile, tile), tile)
            s = mm(k_s[at, :], q, NT)
            if diagonal:
                s = jnp.where(key_seg <= query_seg, s, -1e30)
            s_s[at, :] = s
            dp_s[at, :] = mm(v_s[at, :], go, NT)
            return jnp.maximum(peak, fold(s, jnp.max))

        peak = lax.fori_loop(0, qi, score, jnp.full((8, tile), -1e30, f32))
        peak = score(qi, peak, diagonal=True)
        top = jnp.max(peak, axis=0, keepdims=True) * steep

        def weigh(kb, carry):
            total, mixed = carry
            at = pl.ds(pl.multiple_of(kb * tile, tile), tile)
            p = jnp.exp2(s_s[at, :] * steep - top)
            s_s[at, :] = p
            return total + fold(p, jnp.sum), mixed + fold(p * dp_s[at, :], jnp.sum)

        zero = jnp.zeros((8, tile), f32)
        total, mixed = lax.fori_loop(0, qi + 1, weigh, (zero, zero))
        inverse = 1.0 / jnp.sum(total, axis=0, keepdims=True)
        delta = jnp.sum(mixed, axis=0, keepdims=True) * inverse

        dq_s[...] = jnp.zeros_like(dq_s)

        def spread(kb, _):
            at = pl.ds(pl.multiple_of(kb * tile, tile), tile)
            probs = s_s[at, :] * inverse
            ds = (probs * (dp_s[at, :] - delta)).astype(bf16)
            dv_s[at, :] += mm(probs.astype(bf16), go)
            dk_s[at, :] += mm(ds, q)
            dq_s[...] += mm(kt_s[kb], ds)
            return 0

        lax.fori_loop(0, qi + 1, spread, 0)
        dq = dq_s[...].T * scale
        back = rotate(dq[:, PLAIN_HEAD_WIDTH:], cosine[rows, :half], -sine[rows, :half])
        done = jnp.concatenate([dq[:, :PLAIN_HEAD_WIDTH], back], axis=1).astype(bf16)
        for h in range(heads):
            @pl.when(pid == h)
            def _():
                dq_out[rows, h * WIDTH : (h + 1) * WIDTH] = done
        return 0

    lax.fori_loop(0, blocks, query_block, 0)

    dk = dk_s[...] * scale
    for h in range(heads):
        @pl.when(pid == h)
        def _():
            dkv_out[:, h * PLAIN_HEAD_WIDTH : (h + 1) * PLAIN_HEAD_WIDTH] = dk[
                :, :PLAIN_HEAD_WIDTH
            ].astype(bf16)
            base = heads * PLAIN_HEAD_WIDTH + h * VALUE_HEAD_WIDTH
            dkv_out[:, base : base + VALUE_HEAD_WIDTH] = dv_s[...].astype(bf16)
            if h == 0:
                dr_out[...] = dk[:, PLAIN_HEAD_WIDTH:]
            else:
                dr_out[...] += dk[:, PLAIN_HEAD_WIDTH:]


def attend_backward(arrived, keys, values, k_rope, cosine, sine, heads):
    length = arrived.shape[0]
    tile = 256
    f32 = jnp.float32
    bf16 = jnp.bfloat16

    def whole(a):
        return pl.BlockSpec(a.shape, lambda i: (0,) * len(a.shape))

    outs = (
        jax.ShapeDtypeStruct((length, heads * WIDTH), bf16),
        jax.ShapeDtypeStruct((length, heads * (PLAIN_HEAD_WIDTH + VALUE_HEAD_WIDTH)), bf16),
        jax.ShapeDtypeStruct((length, ROPE), f32),
    )
    ins = (arrived, keys, values, k_rope, cosine, sine)
    return pl.pallas_call(
        functools.partial(attention_kernel, heads, tile),
        grid=(heads,),
        out_shape=outs,
        in_specs=[whole(a) for a in ins],
        out_specs=tuple(whole(a) for a in outs),
        scratch_shapes=[
            pltpu.VMEM((length, WIDTH), bf16),
            pltpu.VMEM((length, VALUE_HEAD_WIDTH), bf16),
            pltpu.VMEM((length, WIDTH), bf16),
            pltpu.VMEM((length // tile, WIDTH, tile), bf16),
            pltpu.VMEM((length, VALUE_HEAD_WIDTH), bf16),
            pltpu.VMEM((length, tile), f32),
            pltpu.VMEM((length, tile), f32),
            pltpu.VMEM((length, WIDTH), f32),
            pltpu.VMEM((length, VALUE_HEAD_WIDTH), f32),
            pltpu.VMEM((WIDTH, tile), f32),
        ],
        compiler_params=pltpu.CompilerParams(
            dimension_semantics=("arbitrary",), vmem_limit_bytes=56 * 1024 * 1024
        ),
        cost_estimate=pl.CostEstimate(
            flops=heads * length * length * 420, bytes_accessed=8 * length * 1024,
            transcendentals=heads * length * length // 2,
        ),
    )(*ins)


def normalise(latent):
    lat = latent.astype(jnp.float32)
    inv_rms = lax.rsqrt(jnp.mean(lat * lat, axis=-1, keepdims=True) + eps)
    return lat * inv_rms, inv_rms


def local(query, latent, rope_key, latent_norm_gain, key_up_matrix, value_up_matrix, out_grad):
    f32 = jnp.float32
    bf16 = jnp.bfloat16
    sp = lax.axis_size("sp")
    dp = lax.axis_size("dp")
    me = lax.axis_index("sp")
    tokens, channels = latent.shape[1:]
    heads = ATTENTION_HEADS // sp
    ratio = sp // dp
    piece = key_up_matrix.shape[0] // sp
    to_user = [
        (s * dp + d, (d * ratio + s // dp) * dp + s % dp) for s in range(sp) for d in range(dp)
    ]
    to_holder = [(b, a) for a, b in to_user]

    packed = jnp.concatenate(
        [
            query[0].reshape(tokens, sp, heads * WIDTH),
            out_grad[0].reshape(tokens, sp, heads * VALUE_HEAD_WIDTH),
        ],
        axis=-1,
    ).transpose(1, 0, 2)
    arrived = lax.all_to_all(packed, "sp", split_axis=0, concat_axis=0, tiled=True)
    arrived = arrived.reshape(sp * tokens, -1)

    fill = LANES - ROPE
    context = jnp.concatenate([latent[0], rope_key[0], jnp.zeros((tokens, fill), bf16)], axis=-1)
    context = lax.all_gather(context, "sp", axis=0, tiled=True)

    rows = jnp.stack(
        [
            lax.dynamic_slice_in_dim(key_up_matrix, me * piece, piece, 0),
            lax.dynamic_slice_in_dim(value_up_matrix, me * piece, piece, 0),
        ]
    )
    rows = lax.ppermute(rows, ("sp", "dp"), to_user)
    weights = lax.all_gather(rows, "dp", axis=1, tiled=True)

    length = sp * tokens
    cosine, sine = angles(length, ROPE)
    normed_all, _ = normalise(context[:, :channels])
    nlat = (normed_all * latent_norm_gain).astype(bf16)
    keys = lax.dot_general(nlat, weights[0], NT, preferred_element_type=f32).astype(bf16)
    values = lax.dot_general(nlat, weights[1], NT, preferred_element_type=f32).astype(bf16)
    k_rope = rotate(context[:, channels : channels + ROPE].astype(f32), cosine, sine).astype(bf16)

    dq, dkv, dr = attend_backward(arrived, keys, values, k_rope, cosine, sine, heads)

    returned = lax.all_to_all(
        dq.reshape(sp, tokens, heads * WIDTH), "sp", split_axis=0, concat_axis=0, tiled=True
    )
    query_grad = returned.transpose(1, 0, 2).reshape(tokens, ATTENTION_HEADS * WIDTH)

    both = weights.reshape(-1, channels)
    d_nlat_part = lax.dot_general(dkv, both, NN, preferred_element_type=f32)
    rope_part = rotate(dr, cosine, -sine)
    sums = jnp.concatenate(
        [d_nlat_part.astype(bf16), rope_part.astype(bf16), jnp.zeros((length, fill), bf16)], axis=-1
    )
    sums = lax.psum_scatter(sums, "sp", scatter_dimension=0, tiled=True)

    weight_part = lax.dot_general(
        dkv, nlat, (((0,), (0,)), ((), ())), preferred_element_type=f32
    ).astype(bf16)
    weight_part = weight_part.reshape(2, -1, channels)
    weight_sum = lax.psum_scatter(weight_part, "dp", scatter_dimension=1, tiled=True)
    weight_sum = lax.ppermute(weight_sum, ("sp", "dp"), to_holder)
    weight_grads = lax.all_gather(weight_sum, "sp", axis=1, tiled=True).astype(f32)

    gain_grad = lax.psum(jnp.sum(d_nlat_part * normed_all, axis=0), ("sp", "dp"))

    normed, inv_rms = normalise(latent[0])
    scaled = sums[:, :channels].astype(f32) * latent_norm_gain
    latent_grad = inv_rms * (scaled - normed * jnp.mean(scaled * normed, axis=-1, keepdims=True))
    rope_grad = sums[:, channels : channels + ROPE].astype(f32)
    return (
        query_grad[None],
        latent_grad[None],
        rope_grad[None],
        weight_grads[0],
        weight_grads[1],
        gain_grad,
    )


def solution(mesh):
    in_specs = (
        P("dp", "sp", None),
        P("dp", "sp", None),
        P("dp", "sp", None),
        P(),
        P("dp", None),
        P("dp", None),
        P("dp", "sp", None),
    )
    out_specs = (
        P("dp", "sp", None),
        P("dp", "sp", None),
        P("dp", "sp", None),
        P("dp", None),
        P("dp", None),
        P(),
    )
    return jax.shard_map(local, mesh=mesh, in_specs=in_specs, out_specs=out_specs, check_vma=False)
```

time: 747 us -> 427 us (0.57); the launches traced: 738 us -> 426 us
  blocking collectives: 171 us -> 67.2 us
  matrix products: 118 us -> 14.6 us
  waiting for transfers between devices: 273 us -> 176 us
  Pallas kernels: 0 us -> 75 us
  local copies, waits for them, and re-layouts: 87 us -> 23.6 us
  other arithmetic: 59.6 us -> 24.6 us
  starting transfers between devices: 15.1 us -> 31.1 us
    all_gather x1 -> x0, blocking collectives: 127 us -> none  [local(): rope_full = lax.all_gather(rope_key[0], 'sp', axis=0, tiled=True)]
    dot_general x27 -> x4, matrix products: 118 us -> 14.6 us  [the longest x1 5.33 us: local(): d_nlat_part = lax.dot_general(dkv, both, NN, preferred_element_type=f32)]
    psum x1 -> x0, waiting for transfers between devices: 103 us -> none  [local(): weight_grads = lax.psum(partial_value, 'sp')]
    all_to_all x3 -> x2, waiting for transfers between devices: 80.7 us -> 0.01 us  [the longest x1 0.01 us: local(): lax.all_to_all(packed, 'sp', split_axis=0, concat_axis=0, tiled=True)]
    reduce_scatter x0 -> x2, waiting for transfers between devices: none -> 78.4 us  [the longest x1 53.5 us: local(): sums = lax.psum_scatter(sums, 'sp', scatter_dimension=0, tiled=True)]
    pallas_call x0 -> x1, Pallas kernels: none -> 75 us  [attend_backward(): pl.pallas_call(functools.partial(attention_kernel, heads, tile), grid=(he...]
    all_gather x2 -> x3, waiting for transfers between devices: 55.1 us -> 97.2 us  [the longest x1 92.3 us: local(): context = lax.all_gather(context, 'sp', axis=0, tiled=True)]
    unnamed x5, waiting for transfers between devices: 34.6 us -> 0.08 us
  transfers between devices with their start and end apart: 7 -> 9, of which waited for: 5 -> 4; matrix products, arithmetic and copies ran while one was open for 10% -> 12% of each run, Pallas kernels for 0% -> 0%
where the time goes in v1:
time: 427 us; the launch traced here: 426 us
  waiting for transfers between devices  176 us (41%)
  Pallas kernels  75 us (18%)
  blocking collectives  67.2 us (16%)
  starting transfers between devices  31.1 us (7%)
  other arithmetic  24.6 us (6%)
  local copies, waits for them, and re-layouts  23.6 us (6%)
  matrix products  14.6 us (3%)
  between operations  13.9 us (3%)
    all_gather x1, waiting for transfers between devices, local(): context = lax.all_gather(context, 'sp', axis=0, tiled=True)  92.3 us
    pallas_call x1, Pallas kernels, attend_backward(): pl.pallas_call(functools.partial(attention_kernel, heads, tile), grid=(he...  75 us
    psum x1, blocking collectives, local(): lax.psum(jnp.sum(d_nlat_part * normed_all, axis=0), ('sp', 'dp'))  67.2 us
    reduce_scatter x1, waiting for transfers between devices, local(): sums = lax.psum_scatter(sums, 'sp', scatter_dimension=0, tiled=True)  53.5 us
    reduce_scatter x1, waiting for transfers between devices, local(): lax.psum_scatter(weight_part, 'dp', scatter_dimension=1, tiled=True)  24.9 us
    all_to_all x1, starting transfers between devices, local(): lax.all_to_all(dq.reshape(sp, tokens, heads * WIDTH), 'sp', split_axis=0,...  19.3 us
  transfers between devices with their start and end apart: 9, of which 4 were waited for; matrix products, arithmetic and copies ran while one was open for 12% of the time, Pallas kernels for 0%

profile of v1, /device:TPU:0, one launch (start us, length us, event | category | flops | bytes accessed | tf_op | source)
XLA Modules:
  0.0 425.7 jit_solution(5428178611434410557)
XLA Ops:
  7.2 0.0 copy-start.2
  7.2 0.0 all-gather.4.cloned.1.call-start
  7.2 0.9 copy.28
  8.2 1.9 concatenate.17
  10.0 0.0 all-gather.4.cloned.1.call-update
  10.0 1.3 copy.36
  11.4 0.2 copy.27
  11.5 0.0 copy-done.2
  11.5 0.2 copy.35
  11.8 0.2 copy.26
  11.9 1.5 maximum_bitcast_fusion
  13.4 7.3 %all-to-all-start = ((bf16[8,192,640]{2,1,0:T(8,128)(2,1)}), bf16[8,192,640]{2,1,0:T(8,128)(2,1)}, u32[]{:S(2)}, u32[]{:S(2)}) async-start(bf16[8,192,640]{2,1,0:T(8,128)(2,1)} %maximum_bitcast_fusion), calls=%async_computation | async-start | bytes 3932160 | tf_op jit(solution)/shard_map/all_to_all | solution.py:227
  20.7 0.0 all-gather.6.cloned.1.call-start
  20.8 1.0 dynamic-slice_bitcast_fusion
  21.8 0.7 collective-permute-start
  22.5 3.8 fusion.12
  26.3 0.0 collective-permute-done
  26.3 0.7 copy-done.3
  27.0 0.0 all-gather.6.cloned.1.call-update
  27.1 0.0 reduce-scatter.5.cloned.1.call-start
  27.1 92.3 %all-gather.4.cloned.1.call-done = bf16[1536,1152]{1,0:T(8,128)(2,1)} async-done(((bf16[192,1152]{1,0:T(8,128)(2,1)}), bf16[1536,1152]{1,0:T(8,128)(2,1)}) %all-gather.4.cloned.1.call-update) | async-done | bytes 3538960 | tf_op jit(solution)/shard_map/all_gather | solution.py:232
  119.4 1.2 slice_convert_fusion
  120.6 0.0 copy-start.4
  120.6 3.9 multiply_subtract_fusion
  124.6 1.8 copy.30
  126.3 1.8 copy.31
  128.1 1.5 pad_maximum_fusion.1
  129.6 1.8 copy.32.k_rope
  131.4 0.0 copy-done.1
  131.4 0.7 fusion.4
  132.1 4.9 %all-gather.6.cloned.1.call-done = bf16[2,256,1024]{2,1,0:T(8,128)(2,1)} async-done(((bf16[2,64,1024]{2,1,0:T(8,128)(2,1)}), bf16[2,256,1024]{2,1,0:T(8,128)(2,1)}) %all-gather.6.cloned.1.call-update) | async-done | bytes 1048592 | tf_op jit(solution)/shard_map/all_gather | solution.py:241
  137.0 0.0 copy-done.4
  137.0 3.1 convolution_convert_fusion.values
  140.1 0.0 copy-done.5
  140.1 2.0 convolution_convert_fusion.1.keys
  142.0 0.0 all-to-all-done
  142.0 75.0 %shard_map.118 = (bf16[1536,384]{1,0:T(8,128)(2,1)}, bf16[1536,512]{1,0:T(8,128)(2,1)}, f32[1536,32]{1,0:T(8,128)}) custom-call(bf16[1536,640]{1,0:T(8,128)(2,1)} %bitcast.1.arrived, bf16[1536,256]{1,0:T(8,128)(2,1)} %convolution_convert_fusion.1.keys, bf16[1536,256]{1,0:T(8,128)(2,1)} %convolution_convert_fusion.values, bf16[1536,32]{1,0:T(8,128)(2,1)} %copy.32.k_rope, ...), custom_call_target="tpu_custom_call" | custom-call | flops 3963617280 | bytes 12582912 | tf_op jit(solution)/shard_map/pallas_call | solution.py:171
  217.0 4.3 %convolution_convert_fusion.2 = bf16[512,1024]{1,0:T(8,128)(2,1)} fusion(bf16[1536,512]{1,0:T(8,128)(2,1)} %get-tuple-element.10, f32[1024]{0:T(1024)S(1)} %copy-done.4, f32[1536]{0:T(1024)S(1)} %add_rsqrt_fusion, bf16[1536,1152]{1,0:T(8,128)(2,1)S(1)} %copy-done.1), kind=kOutput, calls=%fused_computation.12 | convolution fusion | flops 1617428480 | bytes 5779456 | tf_op jit(solution)/shard_map/dot_general | solution.py:266
  221.3 0.0 reduce-scatter.5.cloned.1.call-update
  221.3 0.0 all-gather.8.cloned.1.call-start
  221.3 24.9 %reduce-scatter.5.cloned.1.call-done = bf16[2,64,1024]{2,1,0:T(8,128)(2,1)} async-done(((bf16[2,256,1024]{2,1,0:T(8,128)(2,1)}), bf16[2,64,1024]{2,1,0:T(8,128)(2,1)}) %reduce-scatter.5.cloned.1.call-update) | async-done | bytes 262160 | tf_op jit(solution)/shard_map/reduce_scatter | solution.py:270
  246.2 3.6 collective-permute-start.1
  249.8 0.0 collective-permute-done.1
  249.8 0.0 all-gather.8.cloned.1.call-update
  249.9 0.0 reduce-scatter.3.cloned.1.call-start
  249.9 5.5 %add_convert_fusion = (bf16[1536,16]{1,0:T(8,128)(2,1)}, bf16[1536,16]{1,0:T(8,128)(2,1)}) fusion(f32[1536,32]{1,0:T(8,128)} %get-tuple-element.11, f32[16]{0:T(128)S(1)} %negate_power_fusion), kind=kLoop, calls=%fused_computation.23 | loop fusion | flops 245760 | bytes 294976 | tf_op jit(solution)/shard_map/convert.2
  255.4 5.3 %fusion.3 = (f32[1024]{0:T(1024)S(1)}, bf16[1536,1024]{1,0:T(8,128)(2,1)}) fusion(f32[1536]{0:T(1024)S(1)} %add_rsqrt_fusion, bf16[1536,1152]{1,0:T(8,128)(2,1)S(1)} %copy-done.1, bf16[1536,512]{1,0:T(8,128)(2,1)} %get-tuple-element.10, bf16[512,1024]{1,0:T(8,128)(2,1)} %bitcast.50), kind=kOutput, calls=%fused_computation.5 | convolution fusion | flops 1618476032 | bytes 8923136 | tf_op jit(solution)/shard_map/dot_general | solution.py:259
  260.8 0.1 broadcast_in_dim.23
  260.8 6.7 %concatenate.19 = bf16[1536,1152]{1,0:T(8,128)(2,1)} concatenate(bf16[1536,1024]{1,0:T(8,128)(2,1)} %get-tuple-element.31, bf16[1536,16]{1,0:T(8,128)(2,1)} %get-tuple-element.35, bf16[1536,16]{1,0:T(8,128)(2,1)} %get-tuple-element.34, bf16[1536,96]{1,0:T(8,128)(2,1)S(1)} %broadcast_in_dim.23), dimensions={1} | concatenate | bytes 7077888 | tf_op jit(solution)/shard_map/concatenate | solution.py:261
  267.5 0.0 reduce-scatter.3.cloned.1.call-update
  267.5 19.3 %all-to-all-start.1 = ((bf16[8,192,384]{2,1,0:T(8,128)(2,1)}), bf16[8,192,384]{2,1,0:T(8,128)(2,1)S(1)}, u32[]{:S(2)}, u32[]{:S(2)}) async-start(bf16[8,192,384]{2,1,0:T(8,128)(2,1)} %bitcast.8), calls=%async_computation.1 | async-start | bytes 2359296 | tf_op jit(solution)/shard_map/all_to_all | solution.py:253
  286.9 0.0 copy-done
  286.9 0.2 fusion.11
  287.0 67.2 %psum.7 = f32[1024]{0:T(1024)} all-reduce(f32[1024]{0:T(1024)S(1)} %get-tuple-element.30), channel_id=1, replica_groups=mesh['sp'=8,'dp'=4] {'sp','dp'}, use_global_device_ids=true, to_apply=%region_6.0 | all-reduce | flops 1024 | bytes 8192 | tf_op jit(solution)/shard_map/psum | solution.py:274
  354.2 0.0 all-to-all-done.1
  354.2 0.7 copy.33
  354.9 1.4 broadcast_in_dim_reshape.3
  356.3 2.1 convert_element_type.42
  358.4 2.3 slice_bitcast_fusion
  360.8 53.5 %reduce-scatter.3.cloned.1.call-done = bf16[192,1152]{1,0:T(8,128)(2,1)} async-done(((bf16[1536,1152]{1,0:T(8,128)(2,1)}), bf16[192,1152]{1,0:T(8,128)(2,1)}) %reduce-scatter.3.cloned.1.call-update) | async-done | bytes 442384 | tf_op jit(solution)/shard_map/reduce_scatter | solution.py:264
  414.3 1.3 fusion.7
  415.6 0.8 fusion.15
  416.4 0.7 copy.34
  417.1 2.1 fusion.10
  (11 shorter events, 0.1 us)
Async XLA Ops:
  7.2 4.4 %copy-start.2 = (bf16[1,192,3072]{2,1,0:T(8,128)(2,1)S(1)}, bf16[1,192,3072]{2,1,0:T(8,128)(2,1)}, u32[]{:S(2)}) copy-start(bf16[1,192,3072]{2,1,0:T(8,128)(2,1)} %param.7) | copy-start | bytes 3538948
  7.2 112.2 %all-gather.4.cloned.1.call-start = ((), (), s32[]{:S(2)}) async-start(), calls=%async_computation.4 | async-start | bytes 3981312 | tf_op jit(solution)/shard_map/all_gather | solution.py:232
  13.4 128.6 %all-to-all-start = ((bf16[8,192,640]{2,1,0:T(8,128)(2,1)}), bf16[8,192,640]{2,1,0:T(8,128)(2,1)}, u32[]{:S(2)}, u32[]{:S(2)}) async-start(bf16[8,192,640]{2,1,0:T(8,128)(2,1)} %maximum_bitcast_fusion), calls=%async_computation | async-start | bytes 3932160 | tf_op jit(solution)/shard_map/all_to_all | solution.py:227
  20.7 116.3 %all-gather.6.cloned.1.call-start = ((), (), s32[]{:S(2)}) async-start(), calls=%async_computation.5 | async-start | bytes 1310720 | tf_op jit(solution)/shard_map/all_gather | solution.py:241
  21.8 4.5 %collective-permute-start = (bf16[2,64,1024]{2,1,0:T(8,128)(2,1)S(1)}, bf16[2,64,1024]{2,1,0:T(8,128)(2,1)S(1)}, u32[]{:S(2)}, u32[]{:S(2)}) collective-permute-start(bf16[2,64,1024]{2,1,0:T(8,128)(2,1)S(1)} %pad_maximum_fusion), channel_id=1, source_target_pairs={{0,0},{1,8},{2,16},{3,24},{4,1},{5,9},{6,17},{7,25},{8,2},{9,10},{... | collective-permute-start | bytes 786440 | tf_op jit(solution)/shard_map/ppermute | solution.py:240
  26.3 0.7 copy-start.3
  27.1 219.2 %reduce-scatter.5.cloned.1.call-start = ((), (), s32[]{:S(2)}) async-start(), calls=%async_computation.7 | async-start | bytes 1310720 | tf_op jit(solution)/shard_map/reduce_scatter | solution.py:270
  119.4 12.0 %copy-start.1 = (bf16[1536,1152]{1,0:T(8,128)(2,1)S(1)}, bf16[1536,1152]{1,0:T(8,128)(2,1)}, u32[]{:S(2)}) copy-start(bf16[1536,1152]{1,0:T(8,128)(2,1)} %all-gather.4.cloned.1.call-done) | copy-start | bytes 10616836
  120.6 16.4 %copy-start.4 = (f32[1024]{0:T(1024)S(1)}, f32[1024]{0:T(1024)}, u32[]{:S(2)}) copy-start(f32[1024]{0:T(1024)} %param.10) | copy-start | bytes 12292
  137.0 3.1 copy-start.5
  221.3 135.0 %all-gather.8.cloned.1.call-start = ((), (), s32[]{:S(2)}) async-start(), calls=%async_computation.8 | async-start | bytes 2359296 | tf_op jit(solution)/shard_map/all_gather | solution.py:272
  246.2 3.6 collective-permute-start.1
  249.9 164.4 %reduce-scatter.3.cloned.1.call-start = ((), (), s32[]{:S(2)}) async-start(), calls=%async_computation.6 | async-start | bytes 3981312 | tf_op jit(solution)/shard_map/reduce_scatter | solution.py:264
  267.5 19.3 %copy-start = (bf16[1,192,1024]{2,1,0:T(8,128)(2,1)S(1)}, bf16[1,192,1024]{2,1,0:T(8,128)(2,1)}, u32[]{:S(2)}) copy-start(bf16[1,192,1024]{2,1,0:T(8,128)(2,1)} %param.8) | copy-start | bytes 1179652
  267.5 86.7 %all-to-all-start.1 = ((bf16[8,192,384]{2,1,0:T(8,128)(2,1)}), bf16[8,192,384]{2,1,0:T(8,128)(2,1)S(1)}, u32[]{:S(2)}, u32[]{:S(2)}) async-start(bf16[8,192,384]{2,1,0:T(8,128)(2,1)} %bitcast.8), calls=%async_computation.1 | async-start | bytes 2359296 | tf_op jit(solution)/shard_map/all_to_all | solution.py:253
Sparse Core Ops, SparseCore 0:
  10.7 108.6 all-gather.3
  121.5 15.4 all-gather.5
  221.4 24.7 reduce-scatter.4
  250.0 84.1 all-gather.7
  337.6 76.6 reduce-scatter.2

commit v2 on v1

--- a/solution.py
+++ b/solution.py
@@ -14,7 +14,6 @@
 VALUE_HEAD_WIDTH = 64
 SPAN = 64
 WIDTH = PLAIN_HEAD_WIDTH + ROPE
-LANES = 128
 
 eps = 1e-06
 rope_base = 10000.0
@@ -45,8 +44,8 @@
 
 def attention_kernel(
     heads, tile,
-    arrived, keys, values, k_rope, cosine, sine,
-    dq_out, dkv_out, dr_out,
+    arrived, keyvals, k_rope, cosine, sine,
+    grads_out, dr_out,
     q_s, go_s, k_s, kt_s, v_s, s_s, dp_s, dk_s, dv_s, dq_s,
 ):
     f32 = jnp.float32
@@ -69,10 +68,11 @@
             base = heads * WIDTH + h * VALUE_HEAD_WIDTH
             go_s[...] = arrived[:, base : base + VALUE_HEAD_WIDTH]
             both = jnp.concatenate(
-                [keys[:, h * PLAIN_HEAD_WIDTH : (h + 1) * PLAIN_HEAD_WIDTH], k_rope[...]], axis=1
+                [keyvals[:, h * PLAIN_HEAD_WIDTH : (h + 1) * PLAIN_HEAD_WIDTH], k_rope[...]], axis=1
             )
             k_s[...] = both
-            v_s[...] = values[:, h * VALUE_HEAD_WIDTH : (h + 1) * VALUE_HEAD_WIDTH]
+            base = heads * PLAIN_HEAD_WIDTH + h * VALUE_HEAD_WIDTH
+            v_s[...] = keyvals[:, base : base + VALUE_HEAD_WIDTH]
 
     for b in range(blocks):
         kt_s[b] = k_s[b * tile : (b + 1) * tile, :].astype(f32).T.astype(bf16)
@@ -133,7 +133,7 @@
         for h in range(heads):
             @pl.when(pid == h)
             def _():
-                dq_out[rows, h * WIDTH : (h + 1) * WIDTH] = done
+                grads_out[rows, h * WIDTH : (h + 1) * WIDTH] = done
         return 0
 
     lax.fori_loop(0, blocks, query_block, 0)
@@ -142,18 +142,17 @@
     for h in range(heads):
         @pl.when(pid == h)
         def _():
-            dkv_out[:, h * PLAIN_HEAD_WIDTH : (h + 1) * PLAIN_HEAD_WIDTH] = dk[
-                :, :PLAIN_HEAD_WIDTH
-            ].astype(bf16)
-            base = heads * PLAIN_HEAD_WIDTH + h * VALUE_HEAD_WIDTH
-            dkv_out[:, base : base + VALUE_HEAD_WIDTH] = dv_s[...].astype(bf16)
+            base = heads * WIDTH + h * PLAIN_HEAD_WIDTH
+            grads_out[:, base : base + PLAIN_HEAD_WIDTH] = dk[:, :PLAIN_HEAD_WIDTH].astype(bf16)
+            base = heads * (WIDTH + PLAIN_HEAD_WIDTH) + h * VALUE_HEAD_WIDTH
+            grads_out[:, base : base + VALUE_HEAD_WIDTH] = dv_s[...].astype(bf16)
             if h == 0:
                 dr_out[...] = dk[:, PLAIN_HEAD_WIDTH:]
             else:
                 dr_out[...] += dk[:, PLAIN_HEAD_WIDTH:]
 
 
-def attend_backward(arrived, keys, values, k_rope, cosine, sine, heads):
+def attend_backward(arrived, keyvals, k_rope, cosine, sine, heads):
     length = arrived.shape[0]
     tile = 256
     f32 = jnp.float32
@@ -163,11 +162,10 @@
         return pl.BlockSpec(a.shape, lambda i: (0,) * len(a.shape))
 
     outs = (
-        jax.ShapeDtypeStruct((length, heads * WIDTH), bf16),
-        jax.ShapeDtypeStruct((length, heads * (PLAIN_HEAD_WIDTH + VALUE_HEAD_WIDTH)), bf16),
+        jax.ShapeDtypeStruct((length, heads * (WIDTH + PLAIN_HEAD_WIDTH + VALUE_HEAD_WIDTH)), bf16),
         jax.ShapeDtypeStruct((length, ROPE), f32),
     )
-    ins = (arrived, keys, values, k_rope, cosine, sine)
+    ins = (arrived, keyvals, k_rope, cosine, sine)
     return pl.pallas_call(
         functools.partial(attention_kernel, heads, tile),
         grid=(heads,),
@@ -207,16 +205,17 @@
     bf16 = jnp.bfloat16
     sp = lax.axis_size("sp")
     dp = lax.axis_size("dp")
-    me = lax.axis_index("sp")
     tokens, channels = latent.shape[1:]
     heads = ATTENTION_HEADS // sp
     ratio = sp // dp
-    piece = key_up_matrix.shape[0] // sp
     to_user = [
         (s * dp + d, (d * ratio + s // dp) * dp + s % dp) for s in range(sp) for d in range(dp)
     ]
     to_holder = [(b, a) for a, b in to_user]
 
+    rope_all = lax.all_gather(rope_key[0], "sp", axis=0, tiled=True)
+    stacked = jnp.stack([key_up_matrix, value_up_matrix])
+    whole = lax.all_gather(stacked, "dp", axis=1, tiled=True)
     packed = jnp.concatenate(
         [
             query[0].reshape(tokens, sp, heads * WIDTH),
@@ -224,59 +223,58 @@
         ],
         axis=-1,
     ).transpose(1, 0, 2)
+    packed, rope_all = lax.optimization_barrier((packed, rope_all))
     arrived = lax.all_to_all(packed, "sp", split_axis=0, concat_axis=0, tiled=True)
     arrived = arrived.reshape(sp * tokens, -1)
 
-    fill = LANES - ROPE
-    context = jnp.concatenate([latent[0], rope_key[0], jnp.zeros((tokens, fill), bf16)], axis=-1)
-    context = lax.all_gather(context, "sp", axis=0, tiled=True)
-
-    rows = jnp.stack(
+    normed, inv_rms = normalise(latent[0])
+    nlat = (normed * latent_norm_gain).astype(bf16)
+    key_cols = lax.dot_general(nlat, whole[0], NT, preferred_element_type=f32).astype(bf16)
+    value_cols = lax.dot_general(nlat, whole[1], NT, preferred_element_type=f32).astype(bf16)
+    keyvals = jnp.concatenate(
         [
-            lax.dynamic_slice_in_dim(key_up_matrix, me * piece, piece, 0),
-            lax.dynamic_slice_in_dim(value_up_matrix, me * piece, piece, 0),
-        ]
-    )
-    rows = lax.ppermute(rows, ("sp", "dp"), to_user)
-    weights = lax.all_gather(rows, "dp", axis=1, tiled=True)
+            key_cols.reshape(tokens, sp, heads * PLAIN_HEAD_WIDTH),
+            value_cols.reshape(tokens, sp, heads * VALUE_HEAD_WIDTH),
+        ],
+        axis=-1,
+    ).transpose(1, 0, 2)
+    keyvals = lax.all_to_all(keyvals, "sp", split_axis=0, concat_axis=0, tiled=True)
+    keyvals = keyvals.reshape(sp * tokens, -1)
+
+    nlat_late, whole = lax.optimization_barrier((nlat, whole))
+    nlat_all = lax.all_gather(nlat_late, "sp", axis=0, tiled=True)
 
     length = sp * tokens
     cosine, sine = angles(length, ROPE)
-    normed_all, _ = normalise(context[:, :channels])
-    nlat = (normed_all * latent_norm_gain).astype(bf16)
-    keys = lax.dot_general(nlat, weights[0], NT, preferred_element_type=f32).astype(bf16)
-    values = lax.dot_general(nlat, weights[1], NT, preferred_element_type=f32).astype(bf16)
-    k_rope = rotate(context[:, channels : channels + ROPE].astype(f32), cosine, sine).astype(bf16)
-
-    dq, dkv, dr = attend_backward(arrived, keys, values, k_rope, cosine, sine, heads)
+    k_rope = rotate(rope_all.astype(f32), cosine, sine).astype(bf16)
+
+    grads, dr = attend_backward(arrived, keyvals, k_rope, cosine, sine, heads)
+    split = heads * WIDTH
+    own_keys = heads * PLAIN_HEAD_WIDTH
 
     returned = lax.all_to_all(
-        dq.reshape(sp, tokens, heads * WIDTH), "sp", split_axis=0, concat_axis=0, tiled=True
-    )
-    query_grad = returned.transpose(1, 0, 2).reshape(tokens, ATTENTION_HEADS * WIDTH)
-
-    both = weights.reshape(-1, channels)
-    d_nlat_part = lax.dot_general(dkv, both, NN, preferred_element_type=f32)
-    rope_part = rotate(dr, cosine, -sine)
-    sums = jnp.concatenate(
-        [d_nlat_part.astype(bf16), rope_part.astype(bf16), jnp.zeros((length, fill), bf16)], axis=-1
-    )
-    sums = lax.psum_scatter(sums, "sp", scatter_dimension=0, tiled=True)
-
+        grads.reshape(sp, tokens, -1), "sp", split_axis=0, concat_axis=0, tiled=True
+    )
     weight_part = lax.dot_general(
-        dkv, nlat, (((0,), (0,)), ((), ())), preferred_element_type=f32
+        grads[:, split:], nlat_all, (((0,), (0,)), ((), ())), preferred_element_type=f32
     ).astype(bf16)
     weight_part = weight_part.reshape(2, -1, channels)
     weight_sum = lax.psum_scatter(weight_part, "dp", scatter_dimension=1, tiled=True)
     weight_sum = lax.ppermute(weight_sum, ("sp", "dp"), to_holder)
     weight_grads = lax.all_gather(weight_sum, "sp", axis=1, tiled=True).astype(f32)
 
-    gain_grad = lax.psum(jnp.sum(d_nlat_part * normed_all, axis=0), ("sp", "dp"))
-
-    normed, inv_rms = normalise(latent[0])
-    scaled = sums[:, :channels].astype(f32) * latent_norm_gain
+    rope_parts = rotate(dr, cosine, -sine).reshape(sp, -1, tokens)
+    rope_parts = lax.all_to_all(rope_parts, "sp", split_axis=0, concat_axis=0, tiled=True)
+    rope_grad = jnp.sum(rope_parts, axis=0).reshape(tokens, ROPE)
+
+    query_grad = returned[:, :, :split].transpose(1, 0, 2).reshape(tokens, -1)
+    dk = returned[:, :, split : split + own_keys].transpose(1, 0, 2).reshape(tokens, -1)
+    dv = returned[:, :, split + own_keys :].transpose(1, 0, 2).reshape(tokens, -1)
+    d_nlat = lax.dot_general(dk, whole[0], NN, preferred_element_type=f32)
+    d_nlat = d_nlat + lax.dot_general(dv, whole[1], NN, preferred_element_type=f32)
+    gain_grad = lax.psum(jnp.sum(d_nlat * normed, axis=0), ("sp", "dp"))
+    scaled = d_nlat * latent_norm_gain
     latent_grad = inv_rms * (scaled - normed * jnp.mean(scaled * normed, axis=-1, keepdims=True))
-    rope_grad = sums[:, channels : channels + ROPE].astype(f32)
     return (
         query_grad[None],
         latent_grad[None],

time: 427 us -> 395 us (0.925)
  waiting for transfers between devices: 176 us -> 145 us
  blocking collectives: 67.2 us -> 88.1 us
  starting transfers between devices: 31.1 us -> 18.8 us
  local copies, waits for them, and re-layouts: 23.6 us -> 11.6 us
  matrix products: 14.6 us -> 19.2 us
    all_gather x2, waiting for transfers between devices: 97.2 us -> 18.2 us  [the longest x1 18.2 us: local(): whole = lax.all_gather(stacked, 'dp', axis=1, tiled=True)]
    all_to_all x1 -> x2, waiting for transfers between devices: 0.01 us -> 77.3 us  [the longest x1 45.7 us: local(): lax.all_to_all(keyvals, 'sp', split_axis=0, concat_axis=0, tiled=True)]
    reduce_scatter x1 -> x0, waiting for transfers between devices: 53.5 us -> none  [local(): sums = lax.psum_scatter(sums, 'sp', scatter_dimension=0, tiled=True)]
    all_gather x0 -> x1, blocking collectives: none -> 32.9 us  [local(): rope_all = lax.all_gather(rope_key[0], 'sp', axis=0, tiled=True)]
    all_to_all x1, waiting for transfers between devices: 0.01 us -> 23.8 us  [local(): lax.all_to_all(packed, 'sp', split_axis=0, concat_axis=0, tiled=True)]
    psum x1, blocking collectives: 67.2 us -> 43.8 us  [local(): gain_grad = lax.psum(jnp.sum(d_nlat * normed, axis=0), ('sp', 'dp'))]
    all_to_all x0 -> x1, blocking collectives: none -> 11.4 us  [local(): lax.all_to_all(rope_parts, 'sp', split_axis=0, concat_axis=0, tiled=True)]
    all_to_all x1 -> x2, starting transfers between devices: 19.3 us -> 9.4 us  [the longest x1 5.77 us: local(): lax.all_to_all(keyvals, 'sp', split_axis=0, concat_axis=0, tiled=True)]
  transfers between devices with their start and end apart: 9 -> 8, of which waited for: 4 -> 5; matrix products, arithmetic and copies ran while one was open for 12% -> 11% of each run, Pallas kernels for 0% -> 19%
where the time goes in v2:
time: 395 us; the launch traced here: 394 us
  waiting for transfers between devices  145 us (37%)
  blocking collectives  88.1 us (22%)
  Pallas kernels  74.7 us (19%)
  other arithmetic  22.4 us (6%)
  matrix products  19.2 us (5%)
  starting transfers between devices  18.8 us (5%)
  between operations  14 us (4%)
  local copies, waits for them, and re-layouts  11.6 us (3%)
    pallas_call x1, Pallas kernels, attend_backward(): pl.pallas_call(functools.partial(attention_kernel, heads, tile), grid=(he...  74.7 us
    all_to_all x1, waiting for transfers between devices, local(): lax.all_to_all(keyvals, 'sp', split_axis=0, concat_axis=0, tiled=True)  45.7 us
    psum x1, blocking collectives, local(): gain_grad = lax.psum(jnp.sum(d_nlat * normed, axis=0), ('sp', 'dp'))  43.8 us
    all_gather x1, blocking collectives, local(): rope_all = lax.all_gather(rope_key[0], 'sp', axis=0, tiled=True)  32.9 us
    all_to_all x1, waiting for transfers between devices, local(): lax.all_to_all(grads.reshape(sp, tokens, -1), 'sp', split_axis=0, concat_...  31.6 us
    reduce_scatter x1, waiting for transfers between devices, local(): lax.psum_scatter(weight_part, 'dp', scatter_dimension=1, tiled=True)  26 us
    all_to_all x1, waiting for transfers between devices, local(): lax.all_to_all(packed, 'sp', split_axis=0, concat_axis=0, tiled=True)  23.8 us
    all_gather x1, waiting for transfers between devices, local(): whole = lax.all_gather(stacked, 'dp', axis=1, tiled=True)  18.2 us
  transfers between devices with their start and end apart: 8, of which 5 were waited for; matrix products, arithmetic and copies ran while one was open for 11% of the time, Pallas kernels for 19%

profile of v2, /device:TPU:0, one launch (start us, length us, event | category | flops | bytes accessed | tf_op | source)
XLA Modules:
  0.0 394.1 jit_solution(5427362936669306915)
XLA Ops:
  7.2 0.0 all-gather.5.cloned.1.call-start
  7.2 0.0 copy-start.3
  7.2 3.1 pad_maximum_fusion
  10.3 0.0 all-gather.5.cloned.1.call-update
  10.4 0.2 copy.85
  10.6 0.2 copy.68
  10.7 0.0 copy-start.5
  10.8 0.9 copy-done.2
  11.6 0.2 copy.84
  11.8 0.2 copy.67
  12.0 0.0 copy-done.5
  12.0 0.1 copy.69
  12.1 32.9 %all-gather = bf16[1,1536,32]{2,1,0:T(8,128)(2,1)S(1)} all-gather(bf16[1,192,32]{2,1,0:T(8,128)(2,1)S(1)} %copy.69), channel_id=2, replica_groups=mesh['sp'=8,'dp'=4] {'sp'}, dimensions={1}, use_global_device_ids=true | all-gather | bytes 110592 | tf_op jit(solution)/shard_map/all_gather | solution.py:216
  45.0 1.5 maximum_bitcast_fusion
  46.5 5.7 %all-to-all-start = ((bf16[8,192,640]{2,1,0:T(8,128)(2,1)}), bf16[8,192,640]{2,1,0:T(8,128)(2,1)S(1)}, u32[]{:S(2)}, u32[]{:S(2)}) async-start(bf16[8,192,640]{2,1,0:T(8,128)(2,1)} %maximum_bitcast_fusion), calls=%async_computation | async-start | bytes 3932160 | tf_op jit(solution)/shard_map/all_to_all | solution.py:227
  52.2 0.0 all-gather.7.cloned.1.call-start
  52.2 0.2 fusion.30
  52.4 0.0 copy-done.4
  52.4 0.9 fusion.24
  53.3 18.2 %all-gather.5.cloned.1.call-done = bf16[2,2048,1024]{2,1,0:T(8,128)(2,1)} async-done(((bf16[2,512,1024]{2,1,0:T(8,128)(2,1)}), bf16[2,2048,1024]{2,1,0:T(8,128)(2,1)}) %all-gather.5.cloned.1.call-update) | async-done | bytes 8388624 | tf_op jit(solution)/shard_map/all_gather | solution.py:218
  71.5 0.0 all-gather.7.cloned.1.call-update
  71.5 3.7 fusion.9
  75.2 3.7 fusion.8
  78.9 0.2 copy_bitcast_fusion
  79.1 1.4 maximum_bitcast_fusion.1
  80.5 23.8 %all-to-all-done = bf16[8,192,640]{2,1,0:T(8,128)(2,1)S(1)} async-done(((bf16[8,192,640]{2,1,0:T(8,128)(2,1)}), bf16[8,192,640]{2,1,0:T(8,128)(2,1)S(1)}, u32[]{:S(2)}, u32[]{:S(2)}) %all-to-all-start) | async-done | bytes 1966112 | tf_op jit(solution)/shard_map/all_to_all | solution.py:227
  104.2 5.8 %all-to-all-start.1 = ((bf16[8,192,512]{2,1,0:T(8,128)(2,1)}), bf16[8,192,512]{2,1,0:T(8,128)(2,1)}, u32[]{:S(2)}, u32[]{:S(2)}) async-start(bf16[8,192,512]{2,1,0:T(8,128)(2,1)} %maximum_bitcast_fusion.1), calls=%async_computation.1 | async-start | bytes 3145728 | tf_op jit(solution)/shard_map/all_to_all | solution.py:241
  110.0 0.1 convert_element_type.42
  110.1 3.3 multiply_subtract_fusion.1
  113.4 0.2 copy.74
  113.5 0.2 copy.73
  113.7 0.9 copy.75.k_rope
  114.7 3.7 fusion.33
  118.4 45.7 %all-to-all-done.1 = bf16[8,192,512]{2,1,0:T(8,128)(2,1)} async-done(((bf16[8,192,512]{2,1,0:T(8,128)(2,1)}), bf16[8,192,512]{2,1,0:T(8,128)(2,1)}, u32[]{:S(2)}, u32[]{:S(2)}) %all-to-all-start.1) | async-done | bytes 1572896 | tf_op jit(solution)/shard_map/all_to_all | solution.py:241
  164.1 74.7 %shard_map.118 = (bf16[1536,896]{1,0:T(8,128)(2,1)}, f32[1536,32]{1,0:T(8,128)}) custom-call(bf16[1536,640]{1,0:T(8,128)(2,1)} %bitcast.97, bf16[1536,512]{1,0:T(8,128)(2,1)} %bitcast.10.keyvals, bf16[1536,32]{1,0:T(8,128)(2,1)} %copy.75.k_rope, f32[1536,16]{1,0:T(8,128)} %get-tuple-element.59.cosine, f32[1536,16]{1,0:T(8,128)} %get-tuple-element.58.sine), custom_call_target="tpu_custom_call" | custom-call | flops 3963617280 | bytes 12582912 | tf_op jit(solution)/shard_map/pallas_call | solution.py:169
  238.7 4.8 %multiply_subtract_fusion = (f32[1536,16]{1,0:T(8,128)S(1)}, f32[1536,16]{1,0:T(8,128)S(1)}) fusion(f32[1536,32]{1,0:T(8,128)} %get-tuple-element.16, f32[16]{0:T(128)S(1)} %negate_power_fusion), kind=kLoop, calls=%fused_computation.45 | loop fusion | flops 196608 | bytes 393280 | tf_op jit(solution)/shard_map/sub | solution.py:27
  243.5 0.3 pad_maximum_fusion.1
  243.8 0.3 reshape.94
  244.0 11.4 %all_to_all.20 = f32[8,32,192]{2,1,0:T(8,128)S(1)} all-to-all(f32[8,32,192]{2,1,0:T(8,128)S(1)} %reshape.94), channel_id=1, replica_groups=mesh['sp'=8,'dp'=4] {'sp'}, dimensions={0} | all-to-all | bytes 393216 | tf_op jit(solution)/shard_map/all_to_all | solution.py:267
  255.4 3.6 all-to-all-start.2
  259.1 0.0 reduce-scatter.2.cloned.1.call-start
  259.1 0.0 all-gather.7.cloned.1.call-done
  259.1 5.1 %fusion.12 = bf16[512,1024]{1,0:T(8,128)(2,1)} fusion(bf16[1536,1024]{1,0:T(8,128)(2,1)} %all-gather.7.cloned.1.call-done, bf16[1536,896]{1,0:T(8,128)(2,1)} %get-tuple-element.14), kind=kOutput, calls=%fused_computation.19 | convolution fusion | flops 1611137024 | bytes 5767168 | tf_op jit(solution)/shard_map/dot_general | solution.py:258
  264.3 0.0 reduce-scatter.2.cloned.1.call-update
  264.3 0.0 all-gather.9.cloned.1.call-start
  264.4 26.0 %reduce-scatter.2.cloned.1.call-done = bf16[2,64,1024]{2,1,0:T(8,128)(2,1)} async-done(((bf16[2,256,1024]{2,1,0:T(8,128)(2,1)}), bf16[2,64,1024]{2,1,0:T(8,128)(2,1)}) %reduce-scatter.2.cloned.1.call-update) | async-done | bytes 262160 | tf_op jit(solution)/shard_map/reduce_scatter | solution.py:262
  290.4 3.6 collective-permute-start
  293.9 0.0 collective-permute-done
  293.9 0.0 all-gather.9.cloned.1.call-update
  294.0 0.1 broadcast_in_dim_reshape.7
  294.1 0.7 copy.79
  294.8 31.6 %all-to-all-done.2 = bf16[8,192,896]{2,1,0:T(8,128)(2,1)S(1)} async-done(((bf16[8,192,896]{2,1,0:T(8,128)(2,1)}), bf16[8,192,896]{2,1,0:T(8,128)(2,1)S(1)}, u32[]{:S(2)}, u32[]{:S(2)}) %all-to-all-start.2) | async-done | bytes 2752544 | tf_op jit(solution)/shard_map/all_to_all | solution.py:255
  326.4 0.1 slice_bitcast_fusion.10
  326.5 1.7 copy.76
  328.2 3.0 broadcast_in_dim_reshape.6
  331.2 0.2 slice_bitcast_fusion.12
  331.4 0.1 copy.83
  331.5 0.1 copy.82
  331.6 3.2 fusion.2
  334.8 3.5 fusion.29
  338.3 43.8 %psum.7 = f32[1024]{0:T(1024)} all-reduce(f32[1024]{0:T(1024)S(1)} %get-tuple-element.48), channel_id=1, replica_groups=mesh['sp'=8,'dp'=4] {'sp','dp'}, use_global_device_ids=true, to_apply=%region_5.0 | all-reduce | flops 1024 | bytes 8192 | tf_op jit(solution)/shard_map/psum | solution.py:275
  382.1 1.1 fusion.28
  383.2 2.0 convert_element_type.45
  385.3 2.3 slice_bitcast_fusion.8
  (13 shorter events, 0.1 us)
Async XLA Ops:
  7.2 64.3 %all-gather.5.cloned.1.call-start = ((), (), s32[]{:S(2)}) async-start(), calls=%async_computation.5 | async-start | bytes 10485760 | tf_op jit(solution)/shard_map/all_gather | solution.py:218
  7.2 3.2 copy-start.3
  10.3 1.3 copy-start.2
  10.7 1.3 copy-start.5
  46.5 5.7 %copy-start = (bf16[1,192,1024]{2,1,0:T(8,128)(2,1)S(1)}, bf16[1,192,1024]{2,1,0:T(8,128)(2,1)}, u32[]{:S(2)}) copy-start(bf16[1,192,1024]{2,1,0:T(8,128)(2,1)} %param.8) | copy-start | bytes 1179652
  46.5 5.9 %copy-start.4 = (f32[1024]{0:T(1024)S(1)}, f32[1024]{0:T(1024)}, u32[]{:S(2)}) copy-start(f32[1024]{0:T(1024)} %param.10) | copy-start | bytes 12292
  46.5 57.7 %all-to-all-start = ((bf16[8,192,640]{2,1,0:T(8,128)(2,1)}), bf16[8,192,640]{2,1,0:T(8,128)(2,1)S(1)}, u32[]{:S(2)}, u32[]{:S(2)}) async-start(bf16[8,192,640]{2,1,0:T(8,128)(2,1)} %maximum_bitcast_fusion), calls=%async_computation | async-start | bytes 3932160 | tf_op jit(solution)/shard_map/all_to_all | solution.py:227
  52.2 206.9 %all-gather.7.cloned.1.call-start = ((), (), s32[]{:S(2)}) async-start(), calls=%async_computation.6 | async-start | bytes 3538944 | tf_op jit(solution)/shard_map/all_gather | solution.py:245
  104.2 9.2 %copy-start.1 = (bf16[8,192,640]{2,1,0:T(8,128)(2,1)}, bf16[8,192,640]{2,1,0:T(8,128)(2,1)S(1)}, u32[]{:S(2)}) copy-start(bf16[8,192,640]{2,1,0:T(8,128)(2,1)S(1)} %all-to-all-done) | copy-start | bytes 5898244
  104.2 59.8 %all-to-all-start.1 = ((bf16[8,192,512]{2,1,0:T(8,128)(2,1)}), bf16[8,192,512]{2,1,0:T(8,128)(2,1)}, u32[]{:S(2)}, u32[]{:S(2)}) async-start(bf16[8,192,512]{2,1,0:T(8,128)(2,1)} %maximum_bitcast_fusion.1), calls=%async_computation.1 | async-start | bytes 3145728 | tf_op jit(solution)/shard_map/all_to_all | solution.py:241
  255.4 71.0 %all-to-all-start.2 = ((bf16[8,192,896]{2,1,0:T(8,128)(2,1)}), bf16[8,192,896]{2,1,0:T(8,128)(2,1)S(1)}, u32[]{:S(2)}, u32[]{:S(2)}) async-start(bf16[8,192,896]{2,1,0:T(8,128)(2,1)} %bitcast.96), calls=%async_computation.2 | async-start | bytes 5505024 | tf_op jit(solution)/shard_map/all_to_all | solution.py:255
  259.1 31.3 %reduce-scatter.2.cloned.1.call-start = ((), (), s32[]{:S(2)}) async-start(), calls=%async_computation.7 | async-start | bytes 1310720 | tf_op jit(solution)/shard_map/reduce_scatter | solution.py:262
  264.3 118.9 %all-gather.9.cloned.1.call-start = ((), (), s32[]{:S(2)}) async-start(), calls=%async_computation.8 | async-start | bytes 2359296 | tf_op jit(solution)/shard_map/all_gather | solution.py:264
  290.4 3.6 collective-permute-start
Sparse Core Ops, SparseCore 0:
  10.5 60.9 all-gather.4
  73.7 88.5 all-gather.6
  264.4 25.8 reduce-scatter.1
  294.1 83.5 all-gather.8

commit v3 on v2

--- a/solution.py
+++ b/solution.py
@@ -28,9 +28,9 @@
     )
 
 
-def angles(length, width):
+def angles(positions, width):
     inverse = 1.0 / rope_base ** (jnp.arange(0, width, 2, dtype=jnp.float32) / width)
-    turned = jnp.arange(length, dtype=jnp.float32)[:, None] * inverse[None, :]
+    turned = positions[:, None] * inverse[None, :]
     return (jnp.cos(turned), jnp.sin(turned))
 
 
@@ -44,13 +44,13 @@
 
 def attention_kernel(
     heads, tile,
-    arrived, keyvals, k_rope, cosine, sine,
+    arrived, keyvals, cosine, sine,
     grads_out, dr_out,
     q_s, go_s, k_s, kt_s, v_s, s_s, dp_s, dk_s, dv_s, dq_s,
 ):
     f32 = jnp.float32
     bf16 = jnp.bfloat16
-    length = k_rope.shape[0]
+    length = keyvals.shape[0]
     blocks = length // tile
     scale = WIDTH ** (-0.5)
     steep = scale * math.log2(math.e)
@@ -67,8 +67,13 @@
             q_s[...] = jnp.concatenate([raw[:, :PLAIN_HEAD_WIDTH], turned], axis=1)
             base = heads * WIDTH + h * VALUE_HEAD_WIDTH
             go_s[...] = arrived[:, base : base + VALUE_HEAD_WIDTH]
+            shared = heads * (PLAIN_HEAD_WIDTH + VALUE_HEAD_WIDTH)
             both = jnp.concatenate(
-                [keyvals[:, h * PLAIN_HEAD_WIDTH : (h + 1) * PLAIN_HEAD_WIDTH], k_rope[...]], axis=1
+                [
+                    keyvals[:, h * PLAIN_HEAD_WIDTH : (h + 1) * PLAIN_HEAD_WIDTH],
+                    keyvals[:, shared : shared + ROPE],
+                ],
+                axis=1,
             )
             k_s[...] = both
             base = heads * PLAIN_HEAD_WIDTH + h * VALUE_HEAD_WIDTH
@@ -152,7 +157,7 @@
                 dr_out[...] += dk[:, PLAIN_HEAD_WIDTH:]
 
 
-def attend_backward(arrived, keyvals, k_rope, cosine, sine, heads):
+def attend_backward(arrived, keyvals, cosine, sine, heads):
     length = arrived.shape[0]
     tile = 256
     f32 = jnp.float32
@@ -165,7 +170,7 @@
         jax.ShapeDtypeStruct((length, heads * (WIDTH + PLAIN_HEAD_WIDTH + VALUE_HEAD_WIDTH)), bf16),
         jax.ShapeDtypeStruct((length, ROPE), f32),
     )
-    ins = (arrived, keyvals, k_rope, cosine, sine)
+    ins = (arrived, keyvals, cosine, sine)
     return pl.pallas_call(
         functools.partial(attention_kernel, heads, tile),
         grid=(heads,),
@@ -194,6 +199,71 @@
     )(*ins)
 
 
+def ring_kernel(n, block, out, send, recv, own):
+    half = n // 2
+    me = lax.axis_index("sp")
+    odd = me % 2
+    place = (1 - odd) * (me // 2) + odd * (n - 1 - me // 2)
+
+    def device(p):
+        back = p // half
+        return (1 - back) * (2 * p) + back * (2 * (n - 1 - p) + 1)
+
+    right = device((place + 1) % n)
+    left = device((place + n - 1) % n)
+    barrier = pltpu.get_barrier_semaphore()
+    for other in (left, right):
+        pl.semaphore_signal(
+            barrier, inc=1, device_id={"sp": other}, device_id_type=pl.DeviceIdType.MESH
+        )
+    pl.semaphore_wait(barrier, 2)
+    kept = [
+        pltpu.make_async_copy(block.at[way], out.at[way, me], own.at[way]) for way in range(2)
+    ]
+    for copy in kept:
+        copy.start()
+    for step in range(n - 1):
+        copies = []
+        for way, target in ((0, right), (1, left)):
+            slot = device((place + n - step) % n if way == 0 else (place + step) % n)
+            source = block.at[way] if step == 0 else out.at[way, slot]
+            copies.append(
+                pltpu.make_async_remote_copy(
+                    src_ref=source,
+                    dst_ref=out.at[way, slot],
+                    send_sem=send.at[way, step],
+                    recv_sem=recv.at[way, step],
+                    device_id={"sp": target},
+                    device_id_type=pl.DeviceIdType.MESH,
+                )
+            )
+        for copy in copies:
+            copy.start()
+        for copy in copies:
+            copy.wait()
+    for copy in kept:
+        copy.wait()
+
+
+def ring_gather(block, n):
+    rows, channels = block.shape[1:]
+    gathered = pl.pallas_call(
+        functools.partial(ring_kernel, n),
+        out_shape=jax.ShapeDtypeStruct((2, n, rows, channels), block.dtype),
+        in_specs=[pl.BlockSpec(memory_space=pltpu.VMEM)],
+        out_specs=pl.BlockSpec(memory_space=pltpu.VMEM),
+        scratch_shapes=[
+            pltpu.SemaphoreType.DMA((2, n - 1)),
+            pltpu.SemaphoreType.DMA((2, n - 1)),
+            pltpu.SemaphoreType.DMA((2,)),
+        ],
+        compiler_params=pltpu.CompilerParams(
+            collective_id=0, has_side_effects=True, vmem_limit_bytes=16 * 1024 * 1024
+        ),
+    )(block)
+    return gathered.reshape(2, n * rows, channels)
+
+
 def normalise(latent):
     lat = latent.astype(jnp.float32)
     inv_rms = lax.rsqrt(jnp.mean(lat * lat, axis=-1, keepdims=True) + eps)
@@ -213,7 +283,6 @@
     ]
     to_holder = [(b, a) for a, b in to_user]
 
-    rope_all = lax.all_gather(rope_key[0], "sp", axis=0, tiled=True)
     stacked = jnp.stack([key_up_matrix, value_up_matrix])
     whole = lax.all_gather(stacked, "dp", axis=1, tiled=True)
     packed = jnp.concatenate(
@@ -223,7 +292,6 @@
         ],
         axis=-1,
     ).transpose(1, 0, 2)
-    packed, rope_all = lax.optimization_barrier((packed, rope_all))
     arrived = lax.all_to_all(packed, "sp", split_axis=0, concat_axis=0, tiled=True)
     arrived = arrived.reshape(sp * tokens, -1)
 
@@ -231,10 +299,14 @@
     nlat = (normed * latent_norm_gain).astype(bf16)
     key_cols = lax.dot_general(nlat, whole[0], NT, preferred_element_type=f32).astype(bf16)
     value_cols = lax.dot_general(nlat, whole[1], NT, preferred_element_type=f32).astype(bf16)
+    at = (lax.axis_index("sp") * tokens + jnp.arange(tokens)).astype(f32)
+    near_cosine, near_sine = angles(at, ROPE)
+    k_rope = rotate(rope_key[0].astype(f32), near_cosine, near_sine).astype(bf16)
     keyvals = jnp.concatenate(
         [
             key_cols.reshape(tokens, sp, heads * PLAIN_HEAD_WIDTH),
             value_cols.reshape(tokens, sp, heads * VALUE_HEAD_WIDTH),
+            jnp.broadcast_to(k_rope[:, None, :], (tokens, sp, ROPE)),
         ],
         axis=-1,
     ).transpose(1, 0, 2)
@@ -245,10 +317,9 @@
     nlat_all = lax.all_gather(nlat_late, "sp", axis=0, tiled=True)
 
     length = sp * tokens
-    cosine, sine = angles(length, ROPE)
-    k_rope = rotate(rope_all.astype(f32), cosine, sine).astype(bf16)
-
-    grads, dr = attend_backward(arrived, keyvals, k_rope, cosine, sine, heads)
+    cosine, sine = angles(jnp.arange(length, dtype=f32), ROPE)
+
+    grads, dr = attend_backward(arrived, keyvals, cosine, sine, heads)
     split = heads * WIDTH
     own_keys = heads * PLAIN_HEAD_WIDTH
 
@@ -261,9 +332,12 @@
     weight_part = weight_part.reshape(2, -1, channels)
     weight_sum = lax.psum_scatter(weight_part, "dp", scatter_dimension=1, tiled=True)
     weight_sum = lax.ppermute(weight_sum, ("sp", "dp"), to_holder)
-    weight_grads = lax.all_gather(weight_sum, "sp", axis=1, tiled=True).astype(f32)
-
+    gathered = ring_gather(weight_sum, sp)
+
+    dr, _ = lax.optimization_barrier((dr, weight_part))
     rope_parts = rotate(dr, cosine, -sine).reshape(sp, -1, tokens)
+    gathered, returned, rope_parts = lax.optimization_barrier((gathered, returned, rope_parts))
+    weight_grads = gathered.astype(f32)
     rope_parts = lax.all_to_all(rope_parts, "sp", split_axis=0, concat_axis=0, tiled=True)
     rope_grad = jnp.sum(rope_parts, axis=0).reshape(tokens, ROPE)
 

time: 395 us -> 426 us (1.078)
  Pallas kernels: 74.7 us -> 144 us
  blocking collectives: 88.1 us -> 40.2 us
  starting transfers between devices: 18.8 us -> 26.6 us
  waiting for transfers between devices: 145 us -> 150 us
    pallas_call x0 -> x1, Pallas kernels: none -> 69 us  [ring_gather(): pl.pallas_call(functools.partial(ring_kernel, n), out_shape=jax.ShapeDtyp...]
    all_gather x1 -> x0, blocking collectives: 32.9 us -> none  [local(): rope_all = lax.all_gather(rope_key[0], 'sp', axis=0, tiled=True)]
    all_to_all x1, waiting for transfers between devices: 31.6 us -> 0.01 us  [local(): lax.all_to_all(grads.reshape(sp, tokens, -1), 'sp', split_axis=0, concat_...]
    all_gather x1, waiting for transfers between devices: 18.2 us -> 49.2 us  [local(): whole = lax.all_gather(stacked, 'dp', axis=1, tiled=True)]
    all_to_all x1, waiting for transfers between devices: 45.7 us -> 73.1 us  [local(): lax.all_to_all(keyvals, 'sp', split_axis=0, concat_axis=0, tiled=True)]
    all_to_all x1, waiting for transfers between devices: 23.8 us -> 0.01 us  [local(): lax.all_to_all(packed, 'sp', split_axis=0, concat_axis=0, tiled=True)]
    all_to_all x1 -> x0, blocking collectives: 11.4 us -> none  [local(): lax.all_to_all(rope_parts, 'sp', split_axis=0, concat_axis=0, tiled=True)]
    all_to_all x0 -> x1, starting transfers between devices: none -> 5.58 us  [local(): lax.all_to_all(rope_parts, 'sp', split_axis=0, concat_axis=0, tiled=True)]
  transfers between devices with their start and end apart: 8 -> 8, of which waited for: 5 -> 4; matrix products, arithmetic and copies ran while one was open for 11% -> 8% of each run, Pallas kernels for 19% -> 34%
where the time goes in v3:
time: 426 us; the launch traced here: 425 us
  waiting for transfers between devices  150 us (35%)
  Pallas kernels  144 us (34%)
  blocking collectives  40.2 us (9%)
  starting transfers between devices  26.6 us (6%)
  other arithmetic  19.4 us (5%)
  matrix products  17.5 us (4%)
  between operations  14 us (3%)
  local copies, waits for them, and re-layouts  13.8 us (3%)
    pallas_call x1, Pallas kernels, attend_backward(): pl.pallas_call(functools.partial(attention_kernel, heads, tile), grid=(he...  74.6 us
    all_to_all x1, waiting for transfers between devices, local(): lax.all_to_all(keyvals, 'sp', split_axis=0, concat_axis=0, tiled=True)  73.1 us
    pallas_call x1, Pallas kernels, ring_gather(): pl.pallas_call(functools.partial(ring_kernel, n), out_shape=jax.ShapeDtyp...  69 us
    all_gather x1, waiting for transfers between devices, local(): whole = lax.all_gather(stacked, 'dp', axis=1, tiled=True)  49.2 us
    psum x1, blocking collectives, local(): gain_grad = lax.psum(jnp.sum(d_nlat * normed, axis=0), ('sp', 'dp'))  40.2 us
    reduce_scatter x1, waiting for transfers between devices, local(): lax.psum_scatter(weight_part, 'dp', scatter_dimension=1, tiled=True)  26.3 us
  transfers between devices with their start and end apart: 8, of which 4 were waited for; matrix products, arithmetic and copies ran while one was open for 8% of the time, Pallas kernels for 34%

profile of v3, /device:TPU:0, one launch (start us, length us, event | category | flops | bytes accessed | tf_op | source)
XLA Modules:
  0.0 425.2 jit_solution(4126244319671201698)
XLA Ops:
  7.2 0.0 all-gather.3.cloned.1.call-start
  7.2 0.0 copy-start.6
  7.2 3.1 pad_maximum_fusion
  10.4 0.0 all-gather.3.cloned.1.call-update
  10.4 0.0 copy-start.7
  10.4 0.2 copy.72
  10.6 0.2 copy.58
  10.8 0.7 copy-done.7
  11.5 0.2 copy.73
  11.7 0.2 copy.59
  11.9 1.5 maximum_bitcast_fusion
  13.4 7.4 %all-to-all-start = ((bf16[8,192,640]{2,1,0:T(8,128)(2,1)}), bf16[8,192,640]{2,1,0:T(8,128)(2,1)S(1)}, u32[]{:S(2)}, u32[]{:S(2)}) async-start(bf16[8,192,640]{2,1,0:T(8,128)(2,1)} %maximum_bitcast_fusion), calls=%async_computation | async-start | bytes 3932160 | tf_op jit(solution)/shard_map/all_to_all | solution.py:295
  20.8 0.0 all-gather.5.cloned.1.call-start
  20.9 0.1 fusion.43
  21.1 0.1 copy.60
  21.2 0.2 fusion.30
  21.4 0.9 fusion.24
  22.3 49.2 %all-gather.3.cloned.1.call-done = bf16[2,2048,1024]{2,1,0:T(8,128)(2,1)} async-done(((bf16[2,512,1024]{2,1,0:T(8,128)(2,1)}), bf16[2,2048,1024]{2,1,0:T(8,128)(2,1)}) %all-gather.3.cloned.1.call-update) | async-done | bytes 8388624 | tf_op jit(solution)/shard_map/all_gather | solution.py:287
  71.5 0.0 all-gather.5.cloned.1.call-update
  71.6 3.7 fusion.8
  75.3 3.7 fusion.9
  79.0 0.2 copy_bitcast_fusion
  79.1 0.1 broadcast_in_dim.4
  79.2 1.6 maximum_bitcast_fusion.1
  80.8 0.0 all-to-all-done
  80.8 5.5 %all-to-all-start.1 = ((bf16[8,192,544]{2,1,0:T(8,128)(2,1)}), bf16[8,192,544]{2,1,0:T(8,128)(2,1)}, u32[]{:S(2)}, u32[]{:S(2)}) async-start(bf16[8,192,544]{2,1,0:T(8,128)(2,1)} %maximum_bitcast_fusion.1), calls=%async_computation.1 | async-start | bytes 3932160 | tf_op jit(solution)/shard_map/all_to_all | solution.py:313
  86.3 3.7 fusion.33
  90.1 73.1 %all-to-all-done.1 = bf16[8,192,544]{2,1,0:T(8,128)(2,1)} async-done(((bf16[8,192,544]{2,1,0:T(8,128)(2,1)}), bf16[8,192,544]{2,1,0:T(8,128)(2,1)}, u32[]{:S(2)}, u32[]{:S(2)}) %all-to-all-start.1) | async-done | bytes 1671200 | tf_op jit(solution)/shard_map/all_to_all | solution.py:313
  163.2 74.6 %shard_map.118 = (bf16[1536,896]{1,0:T(8,128)(2,1)}, f32[1536,32]{1,0:T(8,128)}) custom-call(bf16[1536,640]{1,0:T(8,128)(2,1)} %bitcast.101, bf16[1536,544]{1,0:T(8,128)(2,1)} %bitcast.11.keyvals, f32[1536,16]{1,0:T(8,128)} %get-tuple-element.63.cosine, f32[1536,16]{1,0:T(8,128)} %get-tuple-element.62.sine), custom_call_target="tpu_custom_call" | custom-call | flops 3963617280 | bytes 12582912 | tf_op jit(solution)/shard_map/pallas_call | solution.py:174
  237.9 6.4 %all-to-all-start.2 = ((bf16[8,192,896]{2,1,0:T(8,128)(2,1)}), bf16[8,192,896]{2,1,0:T(8,128)(2,1)}, u32[]{:S(2)}, u32[]{:S(2)}) async-start(bf16[8,192,896]{2,1,0:T(8,128)(2,1)} %bitcast.100), calls=%async_computation.3 | async-start | bytes 5505024 | tf_op jit(solution)/shard_map/all_to_all | solution.py:326
  244.3 0.0 reduce-scatter.2.cloned.1.call-start
  244.3 0.0 all-gather.5.cloned.1.call-done
  244.4 4.8 %fusion.12 = bf16[512,1024]{1,0:T(8,128)(2,1)} fusion(bf16[1536,1024]{1,0:T(8,128)(2,1)} %all-gather.5.cloned.1.call-done, bf16[1536,896]{1,0:T(8,128)(2,1)S(1)} %copy-done.4), kind=kOutput, calls=%fused_computation.19 | convolution fusion | flops 1611137024 | bytes 5767168 | tf_op jit(solution)/shard_map/dot_general | solution.py:329
  249.1 0.0 reduce-scatter.2.cloned.1.call-update
  249.1 26.3 %reduce-scatter.2.cloned.1.call-done = bf16[2,64,1024]{2,1,0:T(8,128)(2,1)} async-done(((bf16[2,256,1024]{2,1,0:T(8,128)(2,1)}), bf16[2,64,1024]{2,1,0:T(8,128)(2,1)}) %reduce-scatter.2.cloned.1.call-update) | async-done | bytes 262160 | tf_op jit(solution)/shard_map/reduce_scatter | solution.py:333
  275.4 1.6 collective-permute-start
  277.0 3.2 multiply_subtract_fusion
  280.2 0.3 pad_maximum_fusion.1
  280.5 1.0 reshape.119
  281.5 0.0 collective-permute-done.block
  281.5 69.0 %shard_map.119 = bf16[2,8,64,1024]{3,2,1,0:T(8,128)(2,1)S(1)} custom-call(bf16[2,64,1024]{2,1,0:T(8,128)(2,1)S(1)} %collective-permute-done.block), custom_call_target="tpu_custom_call" | custom-call | tf_op jit(solution)/shard_map/pallas_call | solution.py:250
  350.5 0.0 all-to-all-done.2
  350.5 0.0 slice-start
  350.5 1.7 slice_bitcast_fusion.12
  352.2 1.5 slice_bitcast_fusion.10
  353.7 0.1 copy.71
  353.7 0.0 slice-start.1
  353.8 0.1 copy.70
  353.8 0.0 copy-start.1
  353.9 3.3 fusion.2
  357.2 0.0 slice-done.1
  357.2 0.1 copy-done.1
  357.3 2.0 fusion.29
  359.3 2.4 convert_element_type.61
  361.7 40.2 %psum.7 = f32[1024]{0:T(1024)} all-reduce(f32[1024]{0:T(1024)S(1)} %get-tuple-element.52), channel_id=1, replica_groups=mesh['sp'=8,'dp'=4] {'sp','dp'}, use_global_device_ids=true, to_apply=%region_5.0 | all-reduce | flops 1024 | bytes 8192 | tf_op jit(solution)/shard_map/psum | solution.py:349
  402.0 0.7 copy.64
  402.7 1.4 broadcast_in_dim_reshape.6
  404.0 5.6 %all-to-all-start.3 = ((f32[8,32,192]{2,1,0:T(8,128)}), f32[8,32,192]{2,1,0:T(8,128)S(1)}, u32[]{:S(2)}, u32[]{:S(2)}) async-start(f32[8,32,192]{2,1,0:T(8,128)} %reshape.119), calls=%async_computation.4 | async-start | bytes 524288 | tf_op jit(solution)/shard_map/all_to_all | solution.py:341
  409.6 0.0 copy-done.2
  409.6 2.2 fusion.28
  411.9 4.8 %slice_bitcast_fusion.8 = (f32[512,1024]{1,0:T(8,128)}, f32[512,1024]{1,0:T(8,128)}) fusion(f32[2,512,1024]{2,1,0:T(8,128)} %convert_element_type.61), kind=kLoop, calls=%fused_computation.12 | loop fusion | bytes 8388608 | tf_op jit(solution)/shard_map/squeeze | solution.py:357
  416.7 1.2 all-to-all-done.3
  417.9 0.1 broadcast_in_dim_reshape.7
  418.0 0.7 copy.67
  (23 shorter events, 0.1 us)
Async XLA Ops:
  7.2 64.4 %all-gather.3.cloned.1.call-start = ((), (), s32[]{:S(2)}) async-start(), calls=%async_computation.5 | async-start | bytes 10485760 | tf_op jit(solution)/shard_map/all_gather | solution.py:287
  7.2 3.2 copy-start.6
  10.4 1.1 copy-start.7
  13.4 7.5 %copy-start.9 = (bf16[1,192,32]{1,2,0:T(8,128)(2,1)S(1)}, bf16[1,192,32]{1,2,0:T(8,128)(2,1)}, u32[]{:S(2)}) copy-start(bf16[1,192,32]{1,2,0:T(8,128)(2,1)} %param.9) | copy-start | bytes 36868
  13.4 7.8 %copy-start = (bf16[1,192,1024]{2,1,0:T(8,128)(2,1)S(1)}, bf16[1,192,1024]{2,1,0:T(8,128)(2,1)}, u32[]{:S(2)}) copy-start(bf16[1,192,1024]{2,1,0:T(8,128)(2,1)} %param.8) | copy-start | bytes 1179652
  13.4 8.0 %copy-start.8 = (f32[1024]{0:T(1024)S(1)}, f32[1024]{0:T(1024)}, u32[]{:S(2)}) copy-start(f32[1024]{0:T(1024)} %param.10) | copy-start | bytes 12292
  13.4 67.4 %all-to-all-start = ((bf16[8,192,640]{2,1,0:T(8,128)(2,1)}), bf16[8,192,640]{2,1,0:T(8,128)(2,1)S(1)}, u32[]{:S(2)}, u32[]{:S(2)}) async-start(bf16[8,192,640]{2,1,0:T(8,128)(2,1)} %maximum_bitcast_fusion), calls=%async_computation | async-start | bytes 3932160 | tf_op jit(solution)/shard_map/all_to_all | solution.py:295
  20.8 223.5 %all-gather.5.cloned.1.call-start = ((), (), s32[]{:S(2)}) async-start(), calls=%async_computation.6 | async-start | bytes 3538944 | tf_op jit(solution)/shard_map/all_gather | solution.py:317
  80.8 9.3 %copy-start.5 = (bf16[8,192,640]{2,1,0:T(8,128)(2,1)}, bf16[8,192,640]{2,1,0:T(8,128)(2,1)S(1)}, u32[]{:S(2)}) copy-start(bf16[8,192,640]{2,1,0:T(8,128)(2,1)S(1)} %all-to-all-done) | copy-start | bytes 5898244
  80.8 82.4 %all-to-all-start.1 = ((bf16[8,192,544]{2,1,0:T(8,128)(2,1)}), bf16[8,192,544]{2,1,0:T(8,128)(2,1)}, u32[]{:S(2)}, u32[]{:S(2)}) async-start(bf16[8,192,544]{2,1,0:T(8,128)(2,1)} %maximum_bitcast_fusion.1), calls=%async_computation.1 | async-start | bytes 3932160 | tf_op jit(solution)/shard_map/all_to_all | solution.py:313
  237.9 6.5 %copy-start.4 = (bf16[1536,896]{1,0:T(8,128)(2,1)S(1)}, bf16[1536,896]{1,0:T(8,128)(2,1)}, u32[]{:S(2)}) copy-start(bf16[1536,896]{1,0:T(8,128)(2,1)} %get-tuple-element.14) | copy-start | bytes 8257540
  237.9 112.6 %all-to-all-start.2 = ((bf16[8,192,896]{2,1,0:T(8,128)(2,1)}), bf16[8,192,896]{2,1,0:T(8,128)(2,1)}, u32[]{:S(2)}, u32[]{:S(2)}) async-start(bf16[8,192,896]{2,1,0:T(8,128)(2,1)} %bitcast.100), calls=%async_computation.3 | async-start | bytes 5505024 | tf_op jit(solution)/shard_map/all_to_all | solution.py:326
  244.3 32.8 %copy-start.3 = (f32[1536,32]{1,0:T(8,128)S(1)}, f32[1536,32]{1,0:T(8,128)}, u32[]{:S(2)}) copy-start(f32[1536,32]{1,0:T(8,128)} %get-tuple-element.17) | copy-start | bytes 589828
  244.3 31.2 %reduce-scatter.2.cloned.1.call-start = ((), (), s32[]{:S(2)}) async-start(), calls=%async_computation.7 | async-start | bytes 1310720 | tf_op jit(solution)/shard_map/reduce_scatter | solution.py:333
  275.4 6.1 %collective-permute-start = (bf16[2,64,1024]{2,1,0:T(8,128)(2,1)}, bf16[2,64,1024]{2,1,0:T(8,128)(2,1)S(1)}, u32[]{:S(2)}, u32[]{:S(2)}) collective-permute-start(bf16[2,64,1024]{2,1,0:T(8,128)(2,1)} %reduce-scatter.2.cloned.1.call-done), channel_id=1, source_target_pairs={{0,0},{8,1},{16,2},{24,3},{1,4},{9,5},{17,6},{25,7},{2,8},{10,9},{... | collective-permute-start | bytes 786440 | tf_op jit(solution)/shard_map/ppermute | solution.py:334
  350.5 6.7 %slice-start = ((s8[8388608]{0:T(1024)(128)(4,1)}), s8[4194304]{0:T(1024)(128)(4,1)S(1)}, s32[]{:S(2)}) async-start(s8[8388608]{0:T(1024)(128)(4,1)} %bitcast.111), calls=%async_computation.8 | async-start | bytes 8388608
  353.7 3.5 slice-start.1
  353.8 3.4 copy-start.1
  361.7 47.9 %copy-start.2 = (bf16[1,192,1024]{2,1,0:T(8,128)(2,1)S(1)}, bf16[1,192,1024]{2,1,0:T(8,128)(2,1)}, u32[]{:S(2)}) copy-start(bf16[1,192,1024]{2,1,0:T(8,128)(2,1)} %param.8) | copy-start | bytes 1179652
  404.0 13.8 %all-to-all-start.3 = ((f32[8,32,192]{2,1,0:T(8,128)}), f32[8,32,192]{2,1,0:T(8,128)S(1)}, u32[]{:S(2)}, u32[]{:S(2)}) async-start(f32[8,32,192]{2,1,0:T(8,128)} %reshape.119), calls=%async_computation.4 | async-start | bytes 524288 | tf_op jit(solution)/shard_map/all_to_all | solution.py:341
Sparse Core Ops, SparseCore 0:
  10.5 60.9 all-gather.2
  73.7 92.6 all-gather.4
  249.3 26.1 reduce-scatter.1
